TPU v7x, 256 devices: a whole 4x4x8 slice. The times are simulated.
256 devices in a mesh: fs: 32 (over z, x), tp: 8 (over y, core).
Axes of the slice: x: 4, y: 4, z: 8, core: 2. Of those that a mesh axis runs over, the one named last changes fastest.
Arguments:
- normed_inputs: bfloat16 [196608, 2048], P(('fs', 'tp')), may hold values from -24 to 24
- query_cotangent: bfloat16 [196608, 1024], P(('fs', 'tp')), may hold values from -6 to 6
- head_outputs: bfloat16 [196608, 1024], P(('fs', 'tp')), may hold values from -24 to 24
- output_cotangent: bfloat16 [196608, 2048], P(('fs', 'tp')), may hold values from -6 to 6
- query_weight: float32 [2048, 1024], P('fs', 'tp'), may hold values from -0.125 to 0.125
- out_weight: float32 [1024, 2048], P('fs', 'tp'), may hold values from -0.1875 to 0.1875
- query_basis: bfloat16 [2048, 512], P('fs'), may hold values from -0.125 to 0.125
- out_basis: bfloat16 [1024, 512], P('fs'), may hold values from -0.1875 to 0.1875
- query_mean: float32 [512, 1024], P('fs', 'tp'), may hold values from -6 to 6
- query_square: float32 [512, 1024], P('fs', 'tp'), may hold values from 0.5 to 2
- out_mean: float32 [512, 2048], P('fs', 'tp'), may hold values from -6 to 6
- out_square: float32 [512, 2048], P('fs', 'tp'), may hold values from 0.5 to 2
Outputs:
- query_mean_new: float32 [512, 1024], P('fs', 'tp')
- query_square_new: float32 [512, 1024], P('fs', 'tp')
- query_step: float32 [2048, 1024], P('fs', 'tp')
- query_weight_new: float32 [2048, 1024], P('fs', 'tp')
- query_copy: bfloat16 [2048, 1024], P(None, 'tp')
- out_mean_new: float32 [512, 2048], P('fs', 'tp')
- out_square_new: float32 [512, 2048], P('fs', 'tp')
- out_step: float32 [1024, 2048], P('fs', 'tp')
- out_weight_new: float32 [1024, 2048], P('fs', 'tp')
- out_copy: bfloat16 [1024, 2048], P(None, 'tp')
All inputs are finite; a program needn't handle non-finite values.
Results may differ from a plain program's by a relative error of at most 0.009.
Values may be sent and summed in bfloat16 or wider, within the bound.
A program may use at most 64 MiB of HBM per device.

v0:
```python
import jax
import jax.numpy as jnp
from jax import lax
from jax.sharding import Mesh
from jax.sharding import PartitionSpec as P

FS = ("fs_0", "fs_1")
FS_TP = ("fs_0", "fs_1", "tp")


def whole_of(value, axes, dim):
    whole = value
    for number in range(len(axes) - 1, -1, -1):
        whole = lax.all_gather(whole, axes[number], axis=dim, tiled=True)
    return whole


def summed_rows(terms, axes):
    total = terms.astype(jnp.bfloat16)
    for axis in axes:
        total = lax.psum_scatter(total, axis, scatter_dimension=0, tiled=True)
    return total.astype(jnp.float32)


def cut_along(value, dim, peers):
    before, after = (value.shape[:dim], value.shape[dim + 1 :])
    return jnp.moveaxis(value.reshape(*before, peers, -1, *after), dim, 0)


def sent_and_summed(value, axis, dim):
    peers = lax.axis_size(axis)
    blocks = lax.all_to_all(cut_along(value, dim, peers), axis, 0, 0, tiled=True)
    return jnp.sum(blocks.astype(jnp.float32), axis=0)


def sent_together(arrays, axis, dim, along):
    both = jnp.concatenate(arrays, axis=along)
    whole, at, finished = (lax.all_gather(both, axis, axis=dim, tiled=True), 0, [])
    for a in arrays:
        finished.append(lax.slice_in_dim(whole, at, at + a.shape[along], axis=along))
        at += a.shape[along]
    return tuple(finished)


def sent_to_all(value, axis):
    copies = jnp.broadcast_to(value, (lax.axis_size(axis), *value.shape))
    return lax.all_to_all(copies, axis, split_axis=0, concat_axis=0, tiled=True)


def over_copies(value, axis):
    return sent_to_all(value, axis).sum(axis=0)


def packed_total(arrays, axis):
    ravelled, at, finished = (jnp.concatenate([a.reshape(-1) for a in arrays]), 0, [])
    total = over_copies(ravelled, axis)
    for a in arrays:
        finished.append(total[at : at + a.size].reshape(a.shape))
        at += a.size
    return tuple(finished)


def laid_out(blocks, dim):
    shape = list(blocks.shape[1:])
    shape[dim] *= blocks.shape[0]
    return jnp.moveaxis(blocks, 0, dim).reshape(shape)


def one_gather(arrays, axis, dims):
    ravelled = jnp.concatenate([a.reshape(-1) for a in arrays])
    lines, at, finished = (lax.all_gather(ravelled, axis), 0, [])
    for a, dim in zip(arrays, dims):
        blocks = lines[:, at : at + a.size].reshape(-1, *a.shape)
        finished.append(laid_out(blocks, dim))
        at += a.size
    return tuple(finished)


def moments(reduced, mean, square):
    mean_new = 0.8 * mean + 0.2 * reduced
    square_new = 0.9 * square + 0.1 * reduced * reduced
    direction = mean_new / (jnp.sqrt(square_new) + 1e-08)
    return (mean_new, square_new, direction)


def split_product(left, right):
    contract = (((0,), (0,)), ((), ()))
    high = left.astype(jnp.bfloat16)
    low = (left - high.astype(jnp.float32)).astype(jnp.bfloat16)
    return lax.dot_general(
        high, right, contract, preferred_element_type=jnp.float32
    ) + lax.dot_general(low, right, contract, preferred_element_type=jnp.float32)


def shards(
    normed_inputs,
    query_cotangent,
    head_outputs,
    output_cotangent,
    query_weight,
    out_weight,
    query_basis,
    out_basis,
    query_mean,
    query_square,
    out_mean,
    out_square,
):
    fs_count = lax.axis_size(FS)
    tp_count = lax.axis_size("tp")
    model_rows = normed_inputs.shape[1]
    query_width = query_cotangent.shape[1]
    token_scale = (normed_inputs.shape[0] * fs_count * tp_count) ** (-0.5)
    query_cols = query_weight.shape[1]
    out_cols = out_weight.shape[1]
    rank_rows = query_mean.shape[0]
    query_all, out_all = (whole_of(query_basis, FS, 0), whole_of(out_basis, FS, 0))
    query_left = jnp.dot(normed_inputs, query_all, preferred_element_type=jnp.float32)
    out_left = jnp.dot(head_outputs, out_all, preferred_element_type=jnp.float32)
    query_part = split_product(query_left, query_cotangent)
    out_part = split_product(out_left, output_cotangent)
    reduced = summed_rows(
        jnp.concatenate(
            [
                query_part.reshape(rank_rows * lax.axis_size(FS), tp_count, query_cols),
                out_part.reshape(rank_rows * lax.axis_size(FS), tp_count, out_cols),
            ],
            axis=2,
        ),
        FS,
    )
    summed = sent_and_summed(reduced.astype(jnp.bfloat16), "tp", 1)
    projected = summed[:, 0, :]
    projected = projected * token_scale
    query_reduced = projected[:, :query_cols]
    out_reduced = projected[:, query_cols:]
    query_mean_new, query_square_new, query_direction = moments(
        query_reduced, query_mean, query_square
    )
    out_mean_new, out_square_new, out_direction = moments(out_reduced, out_mean, out_square)
    query_piece, out_piece = sent_together((query_direction, out_direction), FS, 0, 1)
    query_part = query_basis.astype(jnp.float32)
    out_part = out_basis.astype(jnp.float32)
    query_full = jnp.dot(query_part, query_piece, precision=lax.Precision.HIGHEST)
    out_full = jnp.dot(out_part, out_piece, precision=lax.Precision.HIGHEST)
    query_norms, out_norms = packed_total(
        (jnp.sum(query_full * query_full, axis=0), jnp.sum(out_full * out_full, axis=0)), FS
    )
    query_step = query_full * lax.rsqrt(query_norms / model_rows + 0.05)
    out_step = out_full * lax.rsqrt(out_norms / query_width + 0.05)
    query_weight_new = query_weight - 0.01 * query_step
    out_weight_new = out_weight - 0.01 * out_step
    query_copy, out_copy = one_gather(
        (query_weight_new.astype(jnp.bfloat16), out_weight_new.astype(jnp.bfloat16)), FS, (0, 0)
    )
    return (
        query_mean_new,
        query_square_new,
        query_step,
        query_weight_new,
        query_copy,
        out_mean_new,
        out_square_new,
        out_step,
        out_weight_new,
        out_copy,
    )


def solution(mesh):
    split = Mesh(mesh.devices.reshape(8, 4, mesh.shape["tp"]), ("fs_0", "fs_1", "tp"))
    return jax.shard_map(
        shards,
        mesh=split,
        in_specs=(
            P(FS_TP, None),
            P(FS_TP, None),
            P(FS_TP, None),
            P(FS_TP, None),
            P(FS, "tp"),
            P(FS, "tp"),
            P(FS, None),
            P(FS, None),
            P(FS, "tp"),
            P(FS, "tp"),
            P(FS, "tp"),
            P(FS, "tp"),
        ),
        out_specs=(
            P(FS, "tp"),
            P(FS, "tp"),
            P(FS, "tp"),
            P(FS, "tp"),
            P(None, "tp"),
            P(FS, "tp"),
            P(FS, "tp"),
            P(FS, "tp"),
            P(FS, "tp"),
            P(None, "tp"),
        ),
        check_vma=False,
    )
```

profile of v0, /device:TPU:8, one launch (start us, length us, event | category | flops | bytes accessed | tf_op | source)
XLA Modules:
  0.0 348.9 jit_solution(16417232988059884068)
XLA Ops:
  7.2 14.1 %all_gather.23 = bf16[128,512]{1,0:T(8,128)(2,1)} all-gather(bf16[32,512]{1,0:T(8,128)(2,1)} %param.19), channel_id=1, replica_groups=mesh['fs_0'=8,'fs_1'=4,'tp'=8] {'fs_1'}, dimensions={0}, use_global_device_ids=true | all-gather | bytes 163840 | tf_op jit(solution)/shard_map/all_gather | solution.py:14
  21.4 13.2 %all_gather.21 = bf16[256,512]{1,0:T(8,128)(2,1)} all-gather(bf16[64,512]{1,0:T(8,128)(2,1)} %param.18), channel_id=1, replica_groups=mesh['fs_0'=8,'fs_1'=4,'tp'=8] {'fs_1'}, dimensions={0}, use_global_device_ids=true | all-gather | bytes 327680 | tf_op jit(solution)/shard_map/all_gather | solution.py:14
  34.7 26.8 %all-gather.7.cloned.1.call-done = bf16[1024,512]{1,0:T(8,128)(2,1)} async-done(((bf16[128,512]{1,0:T(8,128)(2,1)}), bf16[1024,512]{1,0:T(8,128)(2,1)}) %all-gather.7.cloned.1.call-update) | async-done | bytes 1048592 | tf_op jit(solution)/shard_map/all_gather | solution.py:14
  61.5 2.7 fusion.17
  64.2 1.8 fusion.4
  66.0 1.8 add_convert_fusion
  67.9 1.5 copy.37
  69.3 33.3 %all-gather.5.cloned.1.call-done = bf16[2048,512]{1,0:T(8,128)(2,1)} async-done(((bf16[256,512]{1,0:T(8,128)(2,1)}), bf16[2048,512]{1,0:T(8,128)(2,1)}) %all-gather.5.cloned.1.call-update) | async-done | bytes 2097168 | tf_op jit(solution)/shard_map/all_gather | solution.py:14
  102.6 4.4 %fusion.16 = f32[768,512]{1,0:T(8,128)S(1)} fusion(bf16[768,2048]{1,0:T(8,128)(2,1)} %param.12, bf16[2048,512]{1,0:T(8,128)(2,1)} %all-gather.5.cloned.1.call-done), kind=kOutput, calls=%fused_computation.42 | convolution fusion | flops 1610612736 | bytes 6815744 | tf_op jit(solution)/shard_map/dot_general | solution.py:118
  107.1 1.0 fusion.7
  108.1 1.0 fusion
  109.1 0.2 copy.38
  109.3 1.4 copy-done.1
  110.7 2.1 pad_maximum_fusion
  112.9 45.8 %reduce-scatter.3.cloned.1.call-done = bf16[64,8,384]{2,0,1:T(8,128)(2,1)} async-done(((bf16[512,8,384]{2,0,1:T(8,128)(2,1)}), bf16[64,8,384]{2,0,1:T(8,128)(2,1)}) %reduce-scatter.3.cloned.1.call-update) | async-done | bytes 393232 | tf_op jit(solution)/shard_map/reduce_scatter | solution.py:21
  158.7 25.3 %reduce-scatter.5.cloned.1.call-done = bf16[16,8,384]{2,0,1:T(8,128)(2,1)} async-done(((bf16[64,8,384]{2,0,1:T(8,128)(2,1)}), bf16[16,8,384]{2,0,1:T(8,128)(2,1)}) %reduce-scatter.5.cloned.1.call-update) | async-done | bytes 98320 | tf_op jit(solution)/shard_map/reduce_scatter | solution.py:21
  184.0 9.3 %all_to_all.11 = bf16[8,16,1,384]{3,1,2,0:T(8,128)(2,1)S(1)} all-to-all(bf16[8,16,1,384]{3,1,2,0:T(8,128)(2,1)} %bitcast.36), channel_id=1, replica_groups=mesh['fs_0'=8,'fs_1'=4,'tp'=8] {'tp'}, dimensions={0} | all-to-all | bytes 196608 | tf_op jit(solution)/shard_map/all_to_all | solution.py:32
  193.4 0.6 add_divide_fusion
  194.0 0.6 add_divide_fusion.1
  194.6 49.8 %all_gather.25 = f32[512,384]{1,0:T(8,128)S(1)} all-gather(f32[16,384]{1,0:T(8,128)S(1)} %pad_maximum_fusion.2), channel_id=1, replica_groups=mesh['fs_0'=8,'fs_1'=4,'tp'=8] {'fs_0','fs_1'}, dimensions={0}, use_global_device_ids=true | all-gather | bytes 811008 | tf_op jit(solution)/shard_map/all_gather | solution.py:38
  244.5 0.3 multiply_reduce_fusion
  244.8 0.3 multiply_reduce_fusion.1
  245.1 16.3 %all_to_all.12 = f32[32,1,384]{2,1,0:T(1,128)S(1)} all-to-all(f32[32,1,384]{2,1,0:T(1,128)S(1)} %broadcast_in_dim.2), channel_id=1, replica_groups=mesh['fs_0'=8,'fs_1'=4,'tp'=8] {'fs_0','fs_1'}, dimensions={0} | all-to-all | bytes 98304 | tf_op jit(solution)/shard_map/all_to_all | solution.py:47
  261.4 0.1 reduce_sum.39
  261.5 0.6 convert_bitcast_fusion
  262.2 0.6 convert_bitcast_fusion.1
  262.8 0.6 pad_maximum_fusion.1
  263.4 70.2 %all-gather.9.cloned.1.call-done = bf16[524288]{0:T(1024)(128)(2,1)} async-done(((bf16[16384]{0:T(1024)(128)(2,1)}), bf16[524288]{0:T(1024)(128)(2,1)}) %all-gather.9.cloned.1.call-update) | async-done | bytes 1048592 | tf_op jit(solution)/shard_map/all_gather | solution.py:71
  333.7 2.3 reshape.50
  336.0 2.2 fusion.15
  338.2 2.1 reshape_reshape.6
  340.3 2.1 reshape_reshape.7
  (39 shorter events, 0.4 us)
Async XLA Ops:
  7.2 57.0 %copy-start = (bf16[768,2048]{1,0:T(8,128)(2,1)S(1)}, bf16[768,2048]{1,0:T(8,128)(2,1)}, u32[]{:S(2)}) copy-start(bf16[768,2048]{1,0:T(8,128)(2,1)} %param.15) | copy-start | bytes 9437188
  7.2 54.3 %all-gather.7.cloned.1.call-start = ((), (), s32[]{:S(2)}) async-start(), calls=%async_computation.5 | async-start | bytes 1179648 | tf_op jit(solution)/shard_map/all_gather | solution.py:14
  21.3 81.3 %all-gather.5.cloned.1.call-start = ((), (), s32[]{:S(2)}) async-start(), calls=%async_computation.4 | async-start | bytes 2359296 | tf_op jit(solution)/shard_map/all_gather | solution.py:14
  34.6 124.0 %reduce-scatter.3.cloned.1.call-start = ((), (), s32[]{:S(2)}) async-start(), calls=%async_computation.6 | async-start | bytes 3538944 | tf_op jit(solution)/shard_map/reduce_scatter | solution.py:21
  102.6 4.5 %copy-start.10 = (bf16[768,1024]{1,0:T(8,128)(2,1)S(1)}, bf16[768,1024]{1,0:T(8,128)(2,1)}, u32[]{:S(2)}) copy-start(bf16[768,1024]{1,0:T(8,128)(2,1)} %param.13) | copy-start | bytes 4718596
  109.1 1.6 copy-start.1
  112.7 80.6 %copy-start.6 = (f32[16,256]{1,0:T(8,128)S(1)}, f32[16,256]{1,0:T(8,128)}, u32[]{:S(2)}) copy-start(f32[16,256]{1,0:T(8,128)} %param.23) | copy-start | bytes 49156
  112.7 80.6 %copy-start.7 = (f32[16,256]{1,0:T(8,128)S(1)}, f32[16,256]{1,0:T(8,128)}, u32[]{:S(2)}) copy-start(f32[16,256]{1,0:T(8,128)} %param.22) | copy-start | bytes 49156
  112.7 81.3 %copy-start.8 = (f32[16,128]{1,0:T(8,128)S(1)}, f32[16,128]{1,0:T(8,128)}, u32[]{:S(2)}) copy-start(f32[16,128]{1,0:T(8,128)} %param.21) | copy-start | bytes 24580
  112.7 81.3 %copy-start.9 = (f32[16,128]{1,0:T(8,128)S(1)}, f32[16,128]{1,0:T(8,128)}, u32[]{:S(2)}) copy-start(f32[16,128]{1,0:T(8,128)} %param.20) | copy-start | bytes 24580
  112.8 131.7 %copy-start.3 = (bf16[32,512]{1,0:T(8,128)(2,1)S(1)}, bf16[32,512]{1,0:T(8,128)(2,1)}, u32[]{:S(2)}) copy-start(bf16[32,512]{1,0:T(8,128)(2,1)} %param.19) | copy-start | bytes 98308
  112.8 132.0 %copy-start.2 = (bf16[64,512]{1,0:T(8,128)(2,1)S(1)}, bf16[64,512]{1,0:T(8,128)(2,1)}, u32[]{:S(2)}) copy-start(bf16[64,512]{1,0:T(8,128)(2,1)} %param.18) | copy-start | bytes 196612
  112.8 148.7 %copy-start.4 = (f32[32,256]{1,0:T(8,128)S(1)}, f32[32,256]{1,0:T(8,128)}, u32[]{:S(2)}) copy-start(f32[32,256]{1,0:T(8,128)} %param.17) | copy-start | bytes 98308
  112.8 149.3 %copy-start.5 = (f32[64,128]{1,0:T(8,128)S(1)}, f32[64,128]{1,0:T(8,128)}, u32[]{:S(2)}) copy-start(f32[64,128]{1,0:T(8,128)} %param.16) | copy-start | bytes 98308
  112.8 71.2 %reduce-scatter.5.cloned.1.call-start = ((), (), s32[]{:S(2)}) async-start(), calls=%async_computation.7 | async-start | bytes 491520 | tf_op jit(solution)/shard_map/reduce_scatter | solution.py:21
  158.7 175.0 %all-gather.9.cloned.1.call-start = ((), (), s32[]{:S(2)}) async-start(), calls=%async_computation.8 | async-start | bytes 1081344 | tf_op jit(solution)/shard_map/all_gather | solution.py:71
Sparse Core Ops, SparseCore 0:
  21.5 39.9 all-gather.6
  63.3 39.2 all-gather.4
  112.9 45.6 reduce-scatter.2
  161.0 22.9 reduce-scatter.4
  263.6 70.0 all-gather.8
where the time goes:
time: 349 us
  waiting for transfers between devices  201 us (58%)
  blocking collectives  103 us (30%)
  between operations  14 us (4%)
  matrix products  13.4 us (4%)
  local copies, waits for them, and re-layouts  11.8 us (3%)
  other arithmetic  5.29 us (2%)
    reduce_scatter x2, waiting for transfers between devices, summed_rows(): total = lax.psum_scatter(total, axis, scatter_dimension=0, tiled=True)  71.1 us
    all_gather x1, waiting for transfers between devices, one_gather(): lines, at, finished = (lax.all_gather(ravelled, axis), 0, [])  70.2 us
    all_gather x2, waiting for transfers between devices, whole_of(): whole = lax.all_gather(whole, axes[number], axis=dim, tiled=True)  60.1 us
    all_gather x1, blocking collectives, sent_together(): lax.all_gather(both, axis, axis=dim, tiled=True)  49.8 us
    all_gather x2, blocking collectives, whole_of(): whole = lax.all_gather(whole, axes[number], axis=dim, tiled=True)  27.3 us
    all_to_all x1, blocking collectives, sent_to_all(): return lax.all_to_all(copies, axis, split_axis=0, concat_axis=0, tiled=True)  16.3 us
    all_to_all x1, blocking collectives, sent_and_summed(): lax.all_to_all(cut_along(value, dim, peers), axis, 0, 0, tiled=True)  9.32 us
  transfers between devices with their start and end apart: 5, of which 5 were waited for; matrix products, arithmetic and copies ran while one was open for 2% of the time, Pallas kernels for 0%

commit v1 on v0

v1 whole, which is shorter than its diff:
```python
import functools

import jax
import jax.numpy as jnp
from jax import lax
from jax.experimental import pallas as pl
from jax.experimental.pallas import tpu as pltpu
from jax.sharding import Mesh
from jax.sharding import PartitionSpec as P

FS = ("z", "x")
FS_TP = ("z", "x", "y", "c")
TP = ("y", "c")
MESH = pl.DeviceIdType.MESH
F32 = jnp.float32
BF16 = jnp.bfloat16
LIMIT = 60 * 1024 * 1024


def nearest_first(n):
    return sorted(range(1, n), key=lambda d: (min(d, n - d), d))


def dot(a, b):
    return jnp.dot(a, b, preferred_element_type=F32)


def exchange(sizes, *refs):
    Z, X, Y, token_scale = sizes
    (xin, qcin, hin, ocin, qbin, obin, qw, ow, qm, qs, om, os_,
     qb_out, ob_out, wg_out, dg_out, qm_out, qs_out, om_out, os_out,
     QB, OB, WG, DG, vx, vqc, vh, voc, lot, lqt,
     pso, pro, yso, yro, xso, xro, zso, zro,
     psq, prq, mq, xsq, xrq, zsq, zrq, ysq, yrq,
     loc, snd, rzo, rxo, rzq, rxq, rzw, rzg, one,
     s_pro, s_yro, s_xro, s_zro, s_prq, s_xrq, s_zrq, s_yrq) = refs
    z, x, y, c = (lax.axis_index(name) for name in ("z", "x", "y", "c"))
    other = 1 - c
    fs = z * X + x
    rank_rows, q_cols = qm.shape
    o_cols = om.shape[1]
    q_rows, o_rows = qw.shape[0], ow.shape[0]

    def local(src, dst, number):
        copy = pltpu.make_async_copy(src, dst, loc.at[number])
        copy.start()
        return copy

    def to(src, dst, send, recv, **where):
        copy = pltpu.make_async_remote_copy(
            src_ref=src, dst_ref=dst, send_sem=send, recv_sem=recv, device_id=where, device_id_type=MESH
        )
        copy.start()

    def received(ref, recv):
        pltpu.make_async_remote_copy(
            src_ref=ref, dst_ref=ref, send_sem=snd.at[0], recv_sem=recv, device_id={"c": other}, device_id_type=MESH
        ).wait_recv()

    def sent(ref, send):
        pltpu.make_async_remote_copy(
            src_ref=ref, dst_ref=ref, send_sem=send, recv_sem=one.at[0], device_id={"c": other}, device_id_type=MESH
        ).wait_send()

    def up(at, d, n):
        return lax.rem(at + d, n)

    def down(at, d, n):
        return lax.rem(at + (n - d), n)

    zs, xs, ys = nearest_first(Z), nearest_first(X), nearest_first(Y)

    own_ob = local(obin, OB.at[fs], 0)
    own_qb = local(qbin, QB.at[fs], 1)
    get_h = local(hin, vh, 2)
    get_oc = local(ocin, voc, 3)
    get_x = local(xin, vx, 4)
    get_qc = local(qcin, vqc, 5)
    WG[fs, 0:q_rows, :] = qw[...].astype(BF16)
    for half in range(o_cols // q_cols):
        WG[fs, q_rows + half * o_rows : q_rows + (half + 1) * o_rows, :] = ow[
            :, half * q_cols : (half + 1) * q_cols
        ].astype(BF16)

    barrier = pltpu.get_barrier_semaphore()
    for d in zs:
        pl.semaphore_signal(barrier, inc=1, device_id={"z": up(z, d, Z)}, device_id_type=MESH)
    for d in xs:
        pl.semaphore_signal(barrier, inc=1, device_id={"x": up(x, d, X)}, device_id_type=MESH)
    for d in ys:
        pl.semaphore_signal(barrier, inc=1, device_id={"y": up(y, d, Y)}, device_id_type=MESH)
    pl.semaphore_signal(barrier, inc=1, device_id={"c": other}, device_id_type=MESH)
    pl.semaphore_wait(barrier, len(zs) + len(xs) + len(ys) + 1)

    def send_z(ref, index, send, rz):
        for d in zs:
            to(ref.at[index], ref.at[index], send, rz.at[d - 1], z=up(z, d, Z))

    def send_x(ref, index, send, rx_of):
        for d in xs:
            to(ref.at[index], ref.at[index], send, rx_of(d), x=up(x, d, X))

    def basis_from_z(B, d, send, rz, rx, rd):
        block = down(z, d, Z) * X + x
        received(B.at[block, c], rz.at[d - 1])
        send_x(B, (block, c), send, lambda e: rx.at[d, e - 1])
        to(B.at[block, c], B.at[block, c], send, rd, c=other)

    def basis_from_x(B, send, rx, rd):
        for d in [0] + zs:
            for e in xs:
                block = down(z, d, Z) * X + down(x, e, X)
                received(B.at[block, c], rx.at[d, e - 1])
                to(B.at[block, c], B.at[block, c], send, rd, c=other)

    def basis_whole(B, rd):
        received(B.at[pl.ds(0, Z * X - 1), 0], rd)

    own_ob.wait()
    send_z(OB, (fs, c), snd.at[0], rzo)
    send_x(OB, (fs, c), snd.at[0], lambda e: rxo.at[0, e - 1])
    own_qb.wait()
    send_z(QB, (fs, c), snd.at[1], rzq)
    for d in zs:
        basis_from_z(OB, d, snd.at[0], rzo, rxo, one.at[1])
    send_x(QB, (fs, c), snd.at[1], lambda e: rxq.at[0, e - 1])
    early = zs[: len(zs) // 2 + 1]
    for d in early:
        basis_from_z(QB, d, snd.at[1], rzq, rxq, one.at[2])
    basis_from_x(OB, snd.at[0], rxo, one.at[1])
    basis_whole(OB, one.at[1])
    put_ob = local(OB, ob_out, 6)

    def left(tokens, B, into, tile):
        width = B.shape[3]
        for at in range(0, width, tile):
            rows = B[:, :, :, at : at + tile].reshape(-1, tile)
            into[at : at + tile, :] = dot(tokens[...], rows).astype(BF16).T

    get_h.wait()
    left(vh, OB, lot, 256 if OB.shape[3] % 256 == 0 else OB.shape[3])
    for d in zs[len(early) :]:
        basis_from_z(QB, d, snd.at[1], rzq, rxq, one.at[2])
    get_oc.wait()
    for yy in range(Y):
        at = pl.multiple_of((yy * 2 + other) * o_cols, o_cols)
        pso[yy] = dot(lot[...], voc[:, pl.ds(at, o_cols)]).astype(BF16)
        to(pso.at[yy], pro.at[yy], snd.at[2], s_pro.at[yy], c=other)
    for d in ys + [0]:
        yy = up(y, d, Y)
        at = pl.multiple_of((yy * 2 + c) * o_cols, o_cols)
        mine = dot(lot[...], voc[:, pl.ds(at, o_cols)])
        received(pro.at[yy], s_pro.at[yy])
        yso[d] = (mine + pro[yy].astype(F32)).astype(BF16)
        if d:
            to(yso.at[d], yro.at[d - 1], snd.at[3], s_yro.at[d - 1], y=yy)

    basis_from_x(QB, snd.at[1], rxq, one.at[2])
    basis_whole(QB, one.at[2])
    put_qb = local(QB, qb_out, 7)
    send_z(WG, fs, snd.at[9], rzw)
    get_x.wait()
    left(vx, QB, lqt, 256 if QB.shape[3] % 256 == 0 else QB.shape[3])
    get_qc.wait()
    for yy in range(Y):
        both = dot(lqt[...], vqc[:, yy * 2 * q_cols : (yy + 1) * 2 * q_cols])
        low, high = both[:, :q_cols], both[:, q_cols:]
        psq[yy] = jnp.where(c == 0, high, low).astype(BF16)
        to(psq.at[yy], prq.at[yy], snd.at[4], s_prq.at[yy], c=other)
        mq[yy] = jnp.where(c == 0, low, high)
    for yy in range(Y):
        received(prq.at[yy], s_prq.at[yy])
        both = mq[yy] + prq[yy].astype(F32)
        by_row = both.reshape(Z, X, rank_rows, q_cols).astype(BF16)
        for xx in range(X):
            xsq[xx, :, yy] = by_row[:, xx]
    for d in xs:
        xx = up(x, d, X)
        to(xsq.at[xx], xrq.at[d - 1], snd.at[5], s_xrq.at[d - 1], x=xx)

    total = yso[0].astype(F32)
    for d in ys:
        received(yro.at[d - 1], s_yro.at[d - 1])
        total = total + yro[d - 1].astype(F32)
    by_row = total.astype(BF16).reshape(Z, X, rank_rows, o_cols)
    for xx in range(X):
        xso[xx] = by_row[:, xx]
    for d in xs:
        xx = up(x, d, X)
        to(xso.at[xx], xro.at[d - 1], snd.at[6], s_xro.at[d - 1], x=xx)

    send_x(WG, fs, snd.at[9], lambda e: one.at[3])
    for d in zs:
        block = down(z, d, Z) * X + x
        received(WG.at[block], rzw.at[d - 1])
        send_x(WG, block, snd.at[9], lambda e: one.at[3])

    total = xsq[x].astype(F32)
    for d in xs:
        received(xrq.at[d - 1], s_xrq.at[d - 1])
        total = total + xrq[d - 1].astype(F32)
    zsq[...] = total.astype(BF16)
    for d in zs:
        zz = up(z, d, Z)
        to(zsq.at[zz], zrq.at[d - 1], snd.at[7], s_zrq.at[d - 1], z=zz)

    total = xso[x].astype(F32)
    for d in xs:
        received(xro.at[d - 1], s_xro.at[d - 1])
        total = total + xro[d - 1].astype(F32)
    zso[...] = total.astype(BF16)
    for d in zs:
        zz = up(z, d, Z)
        to(zso.at[zz], zro.at[d - 1], snd.at[8], s_zro.at[d - 1], z=zz)

    total = zsq[z].astype(F32)
    for d in zs:
        received(zrq.at[d - 1], s_zrq.at[d - 1])
        total = total + zrq[d - 1].astype(F32)
    ysq[...] = total.astype(BF16)
    for d in ys:
        yy = up(y, d, Y)
        to(ysq.at[yy], yrq.at[d - 1], snd.at[11], s_yrq.at[d - 1], y=yy)

    def moments(reduced, mean, square, mean_out, square_out):
        mean_new = 0.8 * mean[...] + 0.2 * reduced
        square_new = 0.9 * square[...] + 0.1 * reduced * reduced
        mean_out[...] = mean_new
        square_out[...] = square_new
        return (mean_new / (jnp.sqrt(square_new) + 1e-08)).astype(BF16)

    total = zso[z].astype(F32)
    for d in zs:
        received(zro.at[d - 1], s_zro.at[d - 1])
        total = total + zro[d - 1].astype(F32)
    DG[fs, :, q_cols:] = moments(total * token_scale, om, os_, om_out, os_out)
    total = ysq[y].astype(F32)
    for d in ys:
        received(yrq.at[d - 1], s_yrq.at[d - 1])
        total = total + yrq[d - 1].astype(F32)
    DG[fs, :, :q_cols] = moments(total * token_scale, qm, qs, qm_out, qs_out)

    send_z(DG, fs, snd.at[10], rzg)
    send_x(DG, fs, snd.at[10], lambda e: one.at[4])
    for d in zs:
        block = down(z, d, Z) * X + x
        received(DG.at[block], rzg.at[d - 1])
        send_x(DG, block, snd.at[10], lambda e: one.at[4])

    received(WG.at[pl.ds(0, Z * (X - 1))], one.at[3])
    put_wg = local(WG, wg_out, 8)
    sent(OB.at[pl.ds(0, Z * X - 1)], snd.at[0])
    sent(QB.at[pl.ds(0, Z * X - 1)], snd.at[1])
    sent(pso, snd.at[2])
    sent(yro, snd.at[3])
    sent(psq, snd.at[4])
    sent(xrq, snd.at[5])
    sent(xro, snd.at[6])
    sent(zrq, snd.at[7])
    sent(zro, snd.at[8])
    sent(WG.at[pl.ds(0, Z * X - 1)], snd.at[9])
    sent(yrq, snd.at[11])
    received(DG.at[pl.ds(0, Z * (X - 1))], one.at[4])
    put_dg = local(DG, dg_out, 9)
    sent(DG.at[pl.ds(0, Z * X - 1)], snd.at[10])
    put_ob.wait()
    put_qb.wait()
    put_wg.wait()
    put_dg.wait()


def finish(X, qb_in, ob_in, wg_in, dg_in, qw, ow, qm, qs, om, os_, *refs):
    (q_step, qw_new, q_copy, o_step, ow_new, o_copy, qm_out, qs_out, om_out, os_out,
     QB, OB, WG, DG, qfull, ofull, vqc, voc, sem) = refs
    fs = lax.axis_index("z") * X + lax.axis_index("x")
    copies = []
    for number, (src, dst) in enumerate(((dg_in, DG), (qb_in, QB), (ob_in, OB), (wg_in, WG))):
        copies.append(pltpu.make_async_copy(src, dst, sem.at[number]))
        copies[-1].start()
    q_cols, o_cols = qm.shape[1], om.shape[1]
    q_rows, o_rows = qw.shape[0], ow.shape[0]
    blocks = QB.shape[0]
    for src, dst in ((qm, qm_out), (qs, qs_out), (om, om_out), (os_, os_out)):
        dst[...] = src[...]
    copies[0].wait()
    copies[1].wait()
    rank = QB.shape[3]
    full = dot(QB[...].reshape(-1, rank), DG[:, :, :q_cols].reshape(rank, q_cols))
    qfull[...] = full
    q_scale = lax.rsqrt(jnp.sum(full * full, axis=0, keepdims=True) / (blocks * q_rows) + 0.05)
    copies[2].wait()
    full = dot(OB[...].reshape(-1, rank), DG[:, :, q_cols:].reshape(rank, o_cols))
    ofull[...] = full
    o_scale = lax.rsqrt(jnp.sum(full * full, axis=0, keepdims=True) / (blocks * o_rows) + 0.05)
    copies[3].wait()
    vqc[...] = (
        WG[:, 0:q_rows, :].astype(F32) - 0.01 * (qfull[...] * q_scale).reshape(blocks, q_rows, q_cols)
    ).astype(BF16).reshape(blocks * q_rows, q_cols)
    put_q = pltpu.make_async_copy(vqc, q_copy, sem.at[4])
    put_q.start()
    for half in range(o_cols // q_cols):
        part = slice(half * q_cols, (half + 1) * q_cols)
        rows = slice(q_rows + half * o_rows, q_rows + (half + 1) * o_rows)
        voc[:, part] = (
            WG[:, rows, :].astype(F32) - 0.01 * (ofull[:, part] * o_scale[:, part]).reshape(blocks, o_rows, q_cols)
        ).astype(BF16).reshape(blocks * o_rows, q_cols)
    put_o = pltpu.make_async_copy(voc, o_copy, sem.at[5])
    put_o.start()
    step = qfull[pl.ds(pl.multiple_of(fs * q_rows, q_rows), q_rows), :] * q_scale
    q_step[...] = step
    qw_new[...] = qw[...] - 0.01 * step
    step = ofull[pl.ds(pl.multiple_of(fs * o_rows, o_rows), o_rows), :] * o_scale
    o_step[...] = step
    ow_new[...] = ow[...] - 0.01 * step
    put_q.wait()
    put_o.wait()


def shards(xin, qc, h, oc, qw, ow, qb, ob, qm, qs, om, os_):
    Z, X, Y, C = (lax.axis_size(name) for name in ("z", "x", "y", "c"))
    blocks = Z * X
    tokens, model = xin.shape
    rank = qb.shape[1]
    q_rows, o_rows, rank_rows = qw.shape[0], ow.shape[0], qm.shape[0]
    q_cols, o_cols = qw.shape[1], ow.shape[1]
    wide = h.shape[1]
    token_scale = (tokens * blocks * Y * C) ** (-0.5)
    halves = o_cols // q_cols
    w_rows = q_rows + halves * o_rows
    any_spec = pl.BlockSpec(memory_space=pl.ANY)
    vmem = pl.BlockSpec(memory_space=pltpu.VMEM)
    shape = jax.ShapeDtypeStruct
    qb_shape = (blocks, 2, q_rows // 2, rank)
    ob_shape = (blocks, 2, o_rows // 2, rank)
    wg_shape = (blocks, w_rows, q_cols)
    dg_shape = (blocks, rank_rows, q_cols + o_cols)
    buffer = lambda *dims: pltpu.VMEM(dims, BF16)
    dma = lambda *dims: pltpu.SemaphoreType.DMA(dims)
    outs = pl.pallas_call(
        functools.partial(exchange, (Z, X, Y, token_scale)),
        out_shape=[
            shape(qb_shape, BF16), shape(ob_shape, BF16), shape(wg_shape, BF16), shape(dg_shape, BF16),
            shape(qm.shape, F32), shape(qs.shape, F32), shape(om.shape, F32), shape(os_.shape, F32),
        ],
        in_specs=[any_spec] * 6 + [vmem] * 6,
        out_specs=[any_spec] * 4 + [vmem] * 4,
        scratch_shapes=[
            buffer(*qb_shape), buffer(*ob_shape), buffer(*wg_shape), buffer(*dg_shape),
            buffer(tokens, model), buffer(tokens, wide), buffer(tokens, wide), buffer(tokens, model),
            buffer(rank, tokens), buffer(rank, tokens),
            buffer(Y, rank, o_cols), buffer(Y, rank, o_cols),
            buffer(Y, rank, o_cols), buffer(Y - 1, rank, o_cols),
            buffer(X, Z, rank_rows, o_cols), buffer(X - 1, Z, rank_rows, o_cols),
            buffer(Z, rank_rows, o_cols), buffer(Z - 1, rank_rows, o_cols),
            buffer(Y, rank, q_cols), buffer(Y, rank, q_cols), pltpu.VMEM((Y, rank, q_cols), F32),
            buffer(X, Z, Y, rank_rows, q_cols), buffer(X - 1, Z, Y, rank_rows, q_cols),
            buffer(Z, Y, rank_rows, q_cols), buffer(Z - 1, Y, rank_rows, q_cols),
            buffer(Y, rank_rows, q_cols), buffer(Y - 1, rank_rows, q_cols),
            dma(10), dma(12), dma(Z - 1), dma(Z, X - 1), dma(Z - 1), dma(Z, X - 1), dma(Z - 1), dma(Z - 1), dma(5),
            dma(Y), dma(Y - 1), dma(X - 1), dma(Z - 1), dma(Y), dma(X - 1), dma(Z - 1), dma(Y - 1),
        ],
        compiler_params=pltpu.CompilerParams(collective_id=0, has_side_effects=True, vmem_limit_bytes=LIMIT),
        name="exchange",
    )(
        xin, qc, h, oc, qb.reshape(qb_shape[1:]), ob.reshape(ob_shape[1:]),
        qw, ow, qm, qs, om, os_,
    )
    qb_all, ob_all, wg_all, dg_all, qm_new, qs_new, om_new, os_new = outs
    (q_step, qw_new, q_copy, o_step, ow_new, o_copy, qm_new, qs_new, om_new, os_new) = pl.pallas_call(
        functools.partial(finish, X),
        out_shape=[
            shape(qw.shape, F32), shape(qw.shape, F32), shape((blocks * q_rows, q_cols), BF16),
            shape(ow.shape, F32), shape(ow.shape, F32), shape((blocks * o_rows, o_cols), BF16),
            shape(qm.shape, F32), shape(qs.shape, F32), shape(om.shape, F32), shape(os_.shape, F32),
        ],
        in_specs=[any_spec] * 4 + [vmem] * 6,
        out_specs=[vmem, vmem, any_spec, vmem, vmem, any_spec] + [vmem] * 4,
        scratch_shapes=[
            buffer(*qb_shape), buffer(*ob_shape), buffer(*wg_shape), buffer(*dg_shape),
            pltpu.VMEM((blocks * q_rows, q_cols), F32), pltpu.VMEM((blocks * o_rows, o_cols), F32),
            buffer(blocks * q_rows, q_cols), buffer(blocks * o_rows, o_cols),
            dma(6),
        ],
        compiler_params=pltpu.CompilerParams(vmem_limit_bytes=LIMIT),
        name="finish",
    )(qb_all, ob_all, wg_all, dg_all, qw, ow, qm_new, qs_new, om_new, os_new)
    return (qm_new, qs_new, q_step, qw_new, q_copy, om_new, os_new, o_step, ow_new, o_copy)


def solution(mesh, split=(8, 4, 4, 2)):
    cube = Mesh(mesh.devices.reshape(split), FS_TP)
    tokens = P(FS_TP, None)
    tile = P(FS, TP)
    return jax.shard_map(
        shards,
        mesh=cube,
        in_specs=(tokens,) * 4 + (tile, tile, P(FS, None), P(FS, None)) + (tile,) * 4,
        out_specs=(tile, tile, tile, tile, P(None, TP), tile, tile, tile, tile, P(None, TP)),
        check_vma=False,
    )
```

time: 349 us -> 74.7 us (0.21)
  waiting for transfers between devices: 201 us -> 0 us
  blocking collectives: 103 us -> 0 us
  Pallas kernels: 0 us -> 73 us
  matrix products: 13.4 us -> 0 us
  between operations: 14 us -> 0.65 us
  local copies, waits for them, and re-layouts: 11.8 us -> 0 us
  other arithmetic: 5.29 us -> 0 us
    all_gather x3 -> x0, waiting for transfers between devices: 130 us -> none  [the longest x1 70.2 us: one_gather(): lines, at, finished = (lax.all_gather(ravelled, axis), 0, [])]
    all_gather x3 -> x0, blocking collectives: 77.1 us -> none  [the longest x1 49.8 us: sent_together(): lax.all_gather(both, axis, axis=dim, tiled=True)]
    pallas_call x0 -> x2, Pallas kernels: none -> 73 us  [the longest x1 66.9 us: shards(): pl.pallas_call(functools.partial(exchange, (Z, X, Y, token_scale)), out_s...]
    reduce_scatter x2 -> x0, waiting for transfers between devices: 71.1 us -> none  [summed_rows(): total = lax.psum_scatter(total, axis, scatter_dimension=0, tiled=True)]
    all_to_all x2 -> x0, blocking collectives: 25.6 us -> none  [the longest x1 16.3 us: sent_to_all(): return lax.all_to_all(copies, axis, split_axis=0, concat_axis=0, tiled=True)]
    dot_general x8 -> x0, matrix products: 13.4 us -> none  [the longest x1 4.44 us: shards(): jnp.dot(normed_inputs, query_all, preferred_element_type=jnp.float32)]
    another operation x2 -> x0, local copies, waits for them, and re-layouts: 4.15 us -> none  [laid_out(): return jnp.moveaxis(blocks, 0, dim).reshape(shape)]
  transfers between devices with their start and end apart: 5 -> 0, of which waited for: 5 -> 0; matrix products, arithmetic and copies ran while one was open for 2% -> 0% of each run, Pallas kernels for 0% -> 0%
where the time goes in v1:
time: 74.7 us; the launch traced here: 73.6 us
  Pallas kernels  73 us (98%)
    pallas_call x1, Pallas kernels, shards(): pl.pallas_call(functools.partial(exchange, (Z, X, Y, token_scale)), out_s...  66.9 us
    pallas_call x1, Pallas kernels, shards(): pl.pallas_call(functools.partial(finish, X), out_shape=[shape(qw.shape, F...  6.06 us

profile of v1, /device:TPU:8, one launch (start us, length us, event | category | flops | bytes accessed | tf_op | source)
XLA Modules:
  0.0 73.6 jit_solution(12707139240209085141)
XLA Ops:
  0.6 66.9 %exchange.1 = (bf16[32,2,32,512]{3,2,1,0:T(8,128)(2,1)}, bf16[32,2,16,512]{3,2,1,0:T(8,128)(2,1)}, bf16[32,128,128]{2,1,0:T(8,128)(2,1)}, bf16[32,16,384]{2,1,0:...) custom-call(bf16[768,2048]{1,0:T(8,128)(2,1)} %refs_0_.1, ...), custom_call_target="tpu_custom_call" | custom-call | tf_op jit(solution)/shard_map/exchange/pallas_call | solution.py:339
  67.6 6.1 %finish.1 = (f32[64,128]{1,0:T(8,128)}, f32[64,128]{1,0:T(8,128)}, bf16[2048,128]{1,0:T(8,128)(2,1)}, f32[32,256]{1,0:T(8,128)}, f32[32,256]{1,0:T(8,128)}, /*in...) custom-call(bf16[32,2,32,512]{3,2,1,0:T(8,128)(2,1)} %get-tuple-elem, ...), custom_call_target="tpu_custom_call" | custom-call | tf_op jit(solution)/shard_map/finish/pallas_call | solution.py:369

commit v2 on v1

v2 whole, which is shorter than its diff:
```python
import functools

import jax
import jax.numpy as jnp
from jax import lax
from jax.experimental import pallas as pl
from jax.experimental.pallas import tpu as pltpu
from jax.sharding import Mesh
from jax.sharding import PartitionSpec as P

FS = ("z", "x")
FS_TP = ("z", "x", "y", "c")
TP = ("y", "c")
MESH = pl.DeviceIdType.MESH
F32 = jnp.float32
BF16 = jnp.bfloat16
LIMIT = 60 * 1024 * 1024


def nearest_first(n):
    return sorted(range(1, n), key=lambda d: (min(d, n - d), d))


def dot(a, b):
    return jnp.dot(a, b, preferred_element_type=F32)


def exchange(sizes, *refs):
    Z, X, Y, token_scale = sizes
    (xin, qcin, hin, ocin, qbin, obin, qw_in, ow_in, qm_in, qs_in, om_in, os_in,
     qb_out, ob_out, wg_out, dg_out, qm_out, qs_out, om_out, os_out,
     QB, OB, WG, DG, vx, vqc, vh, voc, lot, lqt, qw, ow, qm, qs, om, os_,
     pso, pro, mo, yso, ror, yro, xso, xro, zso, zro,
     psq, prq, mq, xsp, xrp, ysp, yrp, ysr, yrr, xsr, xrr, zsq, zrq,
     loc, snd, a_send, b_send, rzo, rxo, pro_d, rzq, rxq, prq_d, rzb, rxb, ryb, rgb, pb, rxw, rrw, rlw, rzg, one,
     s_pro, s_yrr, s_yro, s_xro, s_zro, s_prq, s_xrp, s_yrp, s_yrr2, s_xrr, s_zrq) = refs
    z, x, y, c = (lax.axis_index(name) for name in ("z", "x", "y", "c"))
    other = 1 - c
    rank_rows, q_cols = qm.shape
    o_cols = om.shape[1]
    q_rows, o_rows = qw.shape[0], ow.shape[0]

    def local(src, dst, number):
        copy = pltpu.make_async_copy(src, dst, loc.at[number])
        copy.start()
        return copy

    def to(src, dst, send, recv, **where):
        copy = pltpu.make_async_remote_copy(
            src_ref=src, dst_ref=dst, send_sem=send, recv_sem=recv, device_id=where, device_id_type=MESH
        )
        copy.start()

    def received(ref, recv):
        pltpu.make_async_remote_copy(
            src_ref=ref, dst_ref=ref, send_sem=snd.at[0], recv_sem=recv, device_id={"c": other}, device_id_type=MESH
        ).wait_recv()

    def sent(ref, send):
        pltpu.make_async_remote_copy(
            src_ref=ref, dst_ref=ref, send_sem=send, recv_sem=one.at[0], device_id={"c": other}, device_id_type=MESH
        ).wait_send()

    def up(at, d, n):
        return lax.rem(at + d, n)

    def down(at, d, n):
        return lax.rem(at + (n - d), n)

    zs, xs, ys = nearest_first(Z), nearest_first(X), nearest_first(Y)
    groups = [[0]] + [zs[at : at + 2] for at in range(0, len(zs), 2)]

    barrier = pltpu.get_barrier_semaphore()
    for d in zs:
        pl.semaphore_signal(barrier, inc=1, device_id={"z": up(z, d, Z)}, device_id_type=MESH)
    for d in xs:
        pl.semaphore_signal(barrier, inc=1, device_id={"x": up(x, d, X)}, device_id_type=MESH)
    for d in ys:
        pl.semaphore_signal(barrier, inc=1, device_id={"y": up(y, d, Y)}, device_id_type=MESH)
    pl.semaphore_signal(barrier, inc=1, device_id={"c": other}, device_id_type=MESH)

    half_rank = OB.shape[4]
    own = [
        local(src.at[:, pl.ds(half * half_rank, half_rank)], ref.at[z, x, half], number * 2 + half)
        for number, (src, ref) in enumerate(((obin, OB), (qbin, QB)))
        for half in range(2)
    ]
    small = [
        local(src, dst, 8 + number)
        for number, (src, dst) in enumerate(
            ((qw_in, qw), (ow_in, ow), (qm_in, qm), (qs_in, qs), (om_in, om), (os_in, os_))
        )
    ]
    get_h = local(hin, vh, 4)
    get_oc = local(ocin, voc, 5)
    get_x = local(xin, vx, 6)
    get_qc = local(qcin, vqc, 7)
    for copy in small + own:
        copy.wait()
    WG[z, x, 0:q_rows, :] = qw[...].astype(BF16)
    for half in range(o_cols // q_cols):
        WG[z, x, q_rows + half * o_rows : q_rows + (half + 1) * o_rows, :] = ow[
            :, half * q_cols : (half + 1) * q_cols
        ].astype(BF16)
    pl.semaphore_wait(barrier, len(zs) + len(xs) + len(ys) + 1)

    def pieces(ref, d, e, rows):
        return ref.at[down(z, d, Z), down(x, e, X), c, rows]

    class Gather:
        def __init__(self, ref, rows, send, rz, rx, pair):
            self.ref, self.rows, self.send, self.rz, self.rx, self.pair = ref, pl.ds(0, rows), send, rz, rx, pair

        def along_z(self):
            view = self.ref.at[z, x, c, self.rows]
            for d in zs:
                to(view, view, self.send.at[0], self.rz.at[d - 1], z=up(z, d, Z))

        def over(self, view, d):
            to(view, view, self.send.at[3 if d else 2], self.pair.at[d], c=other)

        def along_x(self, d):
            view = pieces(self.ref, d, 0, self.rows)
            if d:
                received(view, self.rz.at[d - 1])
            for e in xs:
                to(view, view, self.send.at[1], self.rx.at[d, e - 1], x=up(x, e, X))
            if d:
                self.over(view, d)

        def arrive(self, d):
            for e in xs:
                view = pieces(self.ref, d, e, self.rows)
                received(view, self.rx.at[d, e - 1])
                self.over(view, d)

        def whole(self):
            for d in [0] + zs:
                block = self.ref.at[0, pl.ds(0, X if d else X - 1), 0, self.rows]
                received(block, self.pair.at[d])

        def done(self):
            sent(self.ref.at[pl.ds(0, Z - 1), 0, 0, self.rows], self.send.at[0])
            sent(self.ref.at[:, pl.ds(0, X - 1), 0, self.rows], self.send.at[1])
            sent(self.ref.at[0, pl.ds(0, X - 1), 0, self.rows], self.send.at[2])
            sent(self.ref.at[pl.ds(0, Z - 1), :, 0, self.rows], self.send.at[3])

    class Shared:
        def __init__(self, ref, first, send):
            self.ref, self.first, self.send = ref, first, send
            self.each = (ref.shape[3] - first) // Y

        def rows(self, yy):
            return pl.ds(pl.multiple_of(self.first + yy * self.each, 8), self.each)

        def group(self, e, yy):
            return self.ref.at[:, down(x, e, X), c, self.rows(yy)]

        def along_z(self):
            view = self.ref.at[z, x, c, self.rows(y)]
            for d in zs:
                to(view, view, self.send.at[0], rzb.at[d - 1], z=up(z, d, Z))

        def along_x(self, d):
            view = pieces(self.ref, d, 0, self.rows(y))
            if d:
                received(view, rzb.at[d - 1])
            for e in xs:
                to(view, view, self.send.at[1], rxb.at[d, e - 1], x=up(x, e, X))
            if d:
                for f in ys:
                    to(view, view, self.send.at[2], ryb.at[d - 1, f - 1], y=up(y, f, Y))
                to(view, view, self.send.at[4], pb.at[0], c=other)

        def along_y(self):
            for e in xs:
                for d in [0] + zs:
                    received(pieces(self.ref, d, e, self.rows(y)), rxb.at[d, e - 1])
                view = self.group(e, y)
                for f in ys:
                    to(view, view, self.send.at[3], rgb.at[e - 1, f - 1], y=up(y, f, Y))
                to(view, view, self.send.at[5], pb.at[1], c=other)

        def arrive(self):
            for d in zs:
                for f in ys:
                    view = pieces(self.ref, d, 0, self.rows(down(y, f, Y)))
                    received(view, ryb.at[d - 1, f - 1])
                    to(view, view, self.send.at[4], pb.at[0], c=other)
            for e in xs:
                for f in ys:
                    view = self.group(e, down(y, f, Y))
                    received(view, rgb.at[e - 1, f - 1])
                    to(view, view, self.send.at[5], pb.at[1], c=other)

        def region(self, grouped, times):
            rows = pl.ds(self.first, times * self.each)
            return self.ref.at[:, pl.ds(0, X - 1), 0, rows] if grouped else self.ref.at[pl.ds(0, Z - 1), 0, 0, rows]

        def whole(self):
            received(self.region(False, Y), pb.at[0])
            received(self.region(True, Y), pb.at[1])

        def done(self):
            for number, (grouped, times) in enumerate(
                ((False, 1), (True, 1), (False, Y - 1), (True, Y - 1), (False, Y), (True, Y))
            ):
                sent(self.region(grouped, times), self.send.at[number])

    class Weights:
        rights, lefts = Z // 2, Z - 1 - Z // 2

        def along_x(self):
            for e in xs:
                to(WG.at[z, x], WG.at[z, x], snd.at[0], rxw.at[e - 1], x=up(x, e, X))

        def step(self, number):
            if number == 1:
                for e in xs:
                    received(WG.at[z, down(x, e, X)], rxw.at[e - 1])
            for count, recv, near, towards in (
                (self.rights, rrw, down(z, number - 1, Z), 1),
                (self.lefts, rlw, up(z, number - 1, Z), Z - 1),
            ):
                if 1 < number <= count + 1:
                    received(WG.at[near], recv.at[number - 2])
                if number <= count:
                    to(WG.at[near], WG.at[near], snd.at[1], recv.at[number - 1], z=up(z, towards, Z))

        def done(self):
            sent(WG.at[0, pl.ds(0, X - 1)], snd.at[0])
            sent(WG.at[pl.ds(0, Z - 1)], snd.at[1])

    gather_o = Gather(OB, o_rows, a_send.at[0], rzo, rxo, pro_d)
    gather_q = Gather(QB, q_rows // 2, a_send.at[1], rzq, rxq, prq_d)
    shared_q = Shared(QB, q_rows // 2, b_send)
    weights = Weights()
    steps = list(range(1, weights.rights + 2))

    def weights_step():
        if steps:
            weights.step(steps.pop(0))

    gather_o.along_z()
    gather_o.along_x(0)
    for number, d in enumerate(zs):
        gather_o.along_x(d)
        if number == min(1, len(zs) - 1):
            shared_q.along_z()
            gather_q.along_z()
    shared_q.along_x(0)
    gather_q.along_x(0)
    for group in groups[1:-1]:
        for d in group:
            shared_q.along_x(d)
            gather_q.along_x(d)
    for group in groups:
        for d in group:
            gather_o.arrive(d)

    def left(tokens, B, into, half):
        rows = B[:, :, half].reshape(-1, half_rank)
        count = tokens.shape[0] // 2
        for part in range(2):
            at = slice(part * count, (part + 1) * count)
            into[half, :, at] = dot(tokens[at], rows).astype(BF16).T

    get_h.wait()
    left(vh, OB, lot, c)
    for d in groups[-1]:
        shared_q.along_x(d)
        gather_q.along_x(d)
    gather_o.whole()
    put_ob = local(OB, ob_out, 14)
    left(vh, OB, lot, other)
    get_oc.wait()
    q_arrivals = list(groups)

    class Ring:
        def __init__(self, axis, at, n, S, R, N, far_send, send, s_r, s_n):
            self.axis, self.at, self.n, self.S, self.R, self.N = axis, at, n, S, R, N
            self.far_send, self.send, self.s_r, self.s_n = far_send, send, s_r, s_n

        def go(self, src, dst, send, recv, d):
            to(src, dst, send, recv, **{self.axis: up(self.at, d, self.n)})

        def far(self, half):
            if self.n == 4:
                self.go(self.S.at[2, half], self.R.at[half], self.far_send, self.s_r.at[half], 3 if half else 1)

        def near(self, d, half):
            last = self.n - 1
            if self.n == 2 or (d, half) in ((1, 1), (last, 0)):
                side = 0 if d == 1 else 1
                self.go(self.S.at[d, half], self.N.at[side, half], self.send, self.s_n.at[side, half], d)

        def merge(self, half):
            if self.n == 4:
                d = 3 if half else 1
                received(self.R.at[half], self.s_r.at[half])
                self.S[d, half] = (self.S[d, half].astype(F32) + self.R[half].astype(F32)).astype(BF16)
                self.go(self.S.at[d, half], self.N.at[half, half], self.send, self.s_n.at[half, half], d)

        def total(self, half):
            result = self.S[0, half].astype(F32)
            for side in range(1 if self.n == 2 else 2):
                received(self.N.at[side, half], self.s_n.at[side, half])
                result = result + self.N[side, half].astype(F32)
            return result

        def done(self):
            if self.n == 4:
                sent(self.R, self.far_send)
                sent(self.N, self.send)
            else:
                sent(self.N.at[0], self.send)

    ring_o = Ring("y", y, Y, yso, ror, yro, snd.at[12], snd.at[3], s_yrr, s_yro)

    rank = 2 * half_rank

    def part_o(number, d):
        yy = up(y, d, Y)
        at = pl.multiple_of(yy * 2 * o_cols, 2 * o_cols)
        both = dot(lot[...].reshape(rank, -1), voc[:, pl.ds(at, 2 * o_cols)])
        low, high = both[:, :o_cols], both[:, o_cols:]
        pso[number] = jnp.where(c == 0, high, low).astype(BF16)
        to(pso.at[number], pro.at[number], snd.at[2], s_pro.at[number], c=other)
        mo[number % 2] = jnp.where(c == 0, low, high)

    def pair_o(number, d):
        received(pro.at[number], s_pro.at[number])
        both = (mo[number % 2] + pro[number].astype(F32)).astype(BF16)
        for half in range(2):
            yso[d, half] = both[half * rank // 2 : (half + 1) * rank // 2]
            if d == 2:
                ring_o.far(half)
            elif d:
                ring_o.near(d, half)

    order = [2, 1, 3, 0] if Y == 4 else [1, 0]
    for number, d in enumerate(order):
        part_o(number, d)
        if number:
            pair_o(number - 1, order[number - 1])
        if number == 0:
            shared_q.along_y()
            weights.along_x()
        elif q_arrivals:
            for e in q_arrivals.pop(0):
                gather_q.arrive(e)
    pair_o(len(order) - 1, order[-1])

    for group in q_arrivals:
        for e in group:
            gather_q.arrive(e)
    weights_step()
    shared_q.arrive()
    get_x.wait()
    left(vx, QB, lqt, c)
    gather_q.whole()
    shared_q.whole()
    put_qb = local(QB, qb_out, 15)
    left(vx, QB, lqt, other)
    get_qc.wait()
    each = Y // 2
    for half in range(2):
        first = half * each
        wide = dot(lqt[...].reshape(rank, -1), vqc[:, first * 2 * q_cols : (first + each) * 2 * q_cols])
        for yy in range(first, first + each):
            at = (yy - first) * 2 * q_cols
            low, high = wide[:, at : at + q_cols], wide[:, at + q_cols : at + 2 * q_cols]
            psq[yy] = jnp.where(c == 0, high, low).astype(BF16)
            to(psq.at[yy], prq.at[yy], snd.at[4], s_prq.at[yy], c=other)
            mq[yy] = jnp.where(c == 0, low, high)
    for half in range(2):
        ring_o.merge(half)
    weights_step()
    low_rows = rank_rows // 2
    for d in ys + [0]:
        yy = up(y, d, Y)
        received(prq.at[yy], s_prq.at[yy])
        both = (mq[yy] + prq[yy].astype(F32)).reshape(Z, X, rank_rows, q_cols)
        for xx in range(X):
            xsp[xx, yy] = both[:, xx, :low_rows].astype(BF16)
            ysr[yy, xx] = both[:, xx, low_rows:].astype(BF16)
        if d:
            to(ysr.at[yy], yrr.at[d - 1], snd.at[5], s_yrr2.at[d - 1], y=yy)
    for d in xs:
        xx = up(x, d, X)
        to(xsp.at[xx], xrp.at[d - 1], snd.at[13], s_xrp.at[d - 1], x=xx)

    per = rank_rows * X
    rows = Z * X // 2
    for half in range(2):
        total = ring_o.total(half).astype(BF16).reshape(rows, rank_rows, o_cols)
        for row in range(rows):
            at = half * rows + row
            xso[at % X, at // X] = total[row]
    for d in xs:
        xx = up(x, d, X)
        to(xso.at[xx], xro.at[d - 1], snd.at[6], s_xro.at[d - 1], x=xx)
    weights_step()

    def summed(own, others, sems):
        total = own.astype(F32)
        for number in range(others.shape[0]):
            received(others.at[number], sems.at[number])
            total = total + others[number].astype(F32)
        return total

    xsr[...] = summed(ysr[y], yrr, s_yrr2).astype(BF16)
    for d in xs:
        xx = up(x, d, X)
        to(xsr.at[xx], xrr.at[d - 1], snd.at[9], s_xrr.at[d - 1], x=xx)
    ysp[...] = summed(xsp[x], xrp, s_xrp).astype(BF16)
    for d in ys:
        yy = up(y, d, Y)
        to(ysp.at[yy], yrp.at[d - 1], snd.at[11], s_yrp.at[d - 1], y=yy)

    total = xso[x].astype(F32)
    for d in xs:
        received(xro.at[d - 1], s_xro.at[d - 1])
        total = total + xro[d - 1].astype(F32)
    zso[...] = total.astype(BF16)
    for d in zs:
        zz = up(z, d, Z)
        to(zso.at[zz], zro.at[d - 1], snd.at[8], s_zro.at[d - 1], z=zz)

    zsq[:, low_rows:] = summed(xsr[x], xrr, s_xrr).astype(BF16)
    zsq[:, :low_rows] = summed(ysp[y], yrp, s_yrp).astype(BF16)
    for d in zs:
        zz = up(z, d, Z)
        to(zsq.at[zz], zrq.at[d - 1], snd.at[7], s_zrq.at[d - 1], z=zz)
    weights_step()

    def moments(reduced, mean, square):
        mean_new = 0.8 * mean[...] + 0.2 * reduced
        square_new = 0.9 * square[...] + 0.1 * reduced * reduced
        mean[...] = mean_new
        square[...] = square_new
        return (mean_new / (jnp.sqrt(square_new) + 1e-08)).astype(BF16)

    total = zso[z].astype(F32)
    for d in zs:
        received(zro.at[d - 1], s_zro.at[d - 1])
        total = total + zro[d - 1].astype(F32)
    DG[z, x, :, q_cols:] = moments(total * token_scale, om, os_)
    total = zsq[z].astype(F32)
    for d in zs:
        received(zrq.at[d - 1], s_zrq.at[d - 1])
        total = total + zrq[d - 1].astype(F32)
    DG[z, x, :, :q_cols] = moments(total * token_scale, qm, qs)

    def direction_x(d):
        view = DG.at[down(z, d, Z), x]
        if d:
            received(view, rzg.at[d - 1])
        for e in xs:
            to(view, view, snd.at[14], one.at[4], x=up(x, e, X))

    for d in zs:
        to(DG.at[z, x], DG.at[z, x], snd.at[10], rzg.at[d - 1], z=up(z, d, Z))
    direction_x(0)
    puts = [
        local(src, dst, number)
        for number, (src, dst) in enumerate(((qm, qm_out), (qs, qs_out), (om, om_out), (os_, os_out)))
    ]
    while steps:
        weights_step()
    for d in zs:
        direction_x(d)

    put_wg = local(WG, wg_out, 4)
    gather_o.done()
    gather_q.done()
    shared_q.done()
    weights.done()
    sent(pso, snd.at[2])
    ring_o.done()
    sent(psq, snd.at[4])
    sent(yrr, snd.at[5])
    sent(xrp, snd.at[13])
    sent(xrr, snd.at[9])
    sent(xro, snd.at[6])
    sent(zrq, snd.at[7])
    sent(zro, snd.at[8])
    sent(yrp, snd.at[11])
    put_ob.wait()
    put_qb.wait()
    for copy in puts:
        copy.wait()
    received(DG.at[:, pl.ds(0, X - 1)], one.at[4])
    put_dg = local(DG, dg_out, 5)
    sent(DG.at[pl.ds(0, Z - 1), 0], snd.at[10])
    sent(DG.at[:, pl.ds(0, X - 1)], snd.at[14])
    put_wg.wait()
    put_dg.wait()


def finish(X, qb_in, ob_in, wg_in, dg_in, qw, ow, qm, qs, om, os_, *refs):
    (q_step, qw_new, q_copy, o_step, ow_new, o_copy, qm_out, qs_out, om_out, os_out,
     QB, OB, WG, DG, qfull, ofull, vqc, voc, sem) = refs
    fs = lax.axis_index("z") * X + lax.axis_index("x")
    copies = []
    for number, (src, dst) in enumerate(((dg_in, DG), (qb_in, QB), (ob_in, OB), (wg_in, WG))):
        copies.append(pltpu.make_async_copy(src, dst, sem.at[number]))
        copies[-1].start()
    q_cols, o_cols = qm.shape[1], om.shape[1]
    q_rows, o_rows = qw.shape[0], ow.shape[0]
    blocks = QB.shape[0] * QB.shape[1]
    for src, dst in ((qm, qm_out), (qs, qs_out), (om, om_out), (os_, os_out)):
        dst[...] = src[...]
    copies[0].wait()
    copies[1].wait()
    half_rank = QB.shape[4]

    def product(B, columns):
        directions = DG[:, :, :, columns].reshape(2 * half_rank, -1)
        return sum(
            dot(B[:, :, half].reshape(-1, half_rank), directions[half * half_rank : (half + 1) * half_rank])
            for half in range(2)
        )

    full = product(QB, slice(0, q_cols))
    qfull[...] = full
    q_scale = lax.rsqrt(jnp.sum(full * full, axis=0, keepdims=True) / (blocks * q_rows) + 0.05)
    copies[2].wait()
    full = product(OB, slice(q_cols, q_cols + o_cols))
    ofull[...] = full
    o_scale = lax.rsqrt(jnp.sum(full * full, axis=0, keepdims=True) / (blocks * o_rows) + 0.05)
    copies[3].wait()
    vqc[...] = (
        WG[:, :, 0:q_rows].reshape(blocks, q_rows, q_cols).astype(F32) - 0.01 * (qfull[...] * q_scale).reshape(blocks, q_rows, q_cols)
    ).astype(BF16).reshape(blocks * q_rows, q_cols)
    put_q = pltpu.make_async_copy(vqc, q_copy, sem.at[4])
    put_q.start()
    for half in range(o_cols // q_cols):
        part = slice(half * q_cols, (half + 1) * q_cols)
        rows = slice(q_rows + half * o_rows, q_rows + (half + 1) * o_rows)
        voc[:, part] = (
            WG[:, :, rows].reshape(blocks, o_rows, q_cols).astype(F32) - 0.01 * (ofull[:, part] * o_scale[:, part]).reshape(blocks, o_rows, q_cols)
        ).astype(BF16).reshape(blocks * o_rows, q_cols)
    put_o = pltpu.make_async_copy(voc, o_copy, sem.at[5])
    put_o.start()
    step = qfull[pl.ds(pl.multiple_of(fs * q_rows, q_rows), q_rows), :] * q_scale
    q_step[...] = step
    qw_new[...] = qw[...] - 0.01 * step
    step = ofull[pl.ds(pl.multiple_of(fs * o_rows, o_rows), o_rows), :] * o_scale
    o_step[...] = step
    ow_new[...] = ow[...] - 0.01 * step
    put_q.wait()
    put_o.wait()


def shards(xin, qc, h, oc, qw, ow, qb, ob, qm, qs, om, os_):
    Z, X, Y, C = (lax.axis_size(name) for name in ("z", "x", "y", "c"))
    blocks = Z * X
    tokens, model = xin.shape
    rank = qb.shape[1]
    q_rows, o_rows, rank_rows = qw.shape[0], ow.shape[0], qm.shape[0]
    q_cols, o_cols = qw.shape[1], ow.shape[1]
    wide = h.shape[1]
    token_scale = (tokens * blocks * Y * C) ** (-0.5)
    halves = o_cols // q_cols
    w_rows = q_rows + halves * o_rows
    any_spec = pl.BlockSpec(memory_space=pl.ANY)
    vmem = pl.BlockSpec(memory_space=pltpu.VMEM)
    shape = jax.ShapeDtypeStruct
    qb_shape = (Z, X, 2, q_rows, rank // 2)
    ob_shape = (Z, X, 2, o_rows, rank // 2)
    wg_shape = (Z, X, w_rows, q_cols)
    dg_shape = (Z, X, rank_rows, q_cols + o_cols)
    near_z = max(Z - 1, 1)
    part_x = (X, Z, rank_rows // 2, q_cols)
    part_y = (Y, Z, rank_rows // 2, q_cols)
    buffer = lambda *dims: pltpu.VMEM(dims, BF16)
    dma = lambda *dims: pltpu.SemaphoreType.DMA(dims)
    outs = pl.pallas_call(
        functools.partial(exchange, (Z, X, Y, token_scale)),
        out_shape=[
            shape(qb_shape, BF16), shape(ob_shape, BF16), shape(wg_shape, BF16), shape(dg_shape, BF16),
            shape(qm.shape, F32), shape(qs.shape, F32), shape(om.shape, F32), shape(os_.shape, F32),
        ],
        in_specs=[any_spec] * 12,
        out_specs=[any_spec] * 8,
        scratch_shapes=[
            buffer(*qb_shape), buffer(*ob_shape), buffer(*wg_shape), buffer(*dg_shape),
            buffer(tokens, model), buffer(tokens, wide), buffer(tokens, wide), buffer(tokens, model),
            buffer(2, rank // 2, tokens), buffer(2, rank // 2, tokens),
            pltpu.VMEM(qw.shape, F32), pltpu.VMEM(ow.shape, F32), pltpu.VMEM(qm.shape, F32),
            pltpu.VMEM(qs.shape, F32), pltpu.VMEM(om.shape, F32), pltpu.VMEM(os_.shape, F32),
            buffer(Y, rank, o_cols), buffer(Y, rank, o_cols), pltpu.VMEM((2, rank, o_cols), F32),
            buffer(Y, 2, rank // 2, o_cols), buffer(2, rank // 2, o_cols), buffer(2, 2, rank // 2, o_cols),
            buffer(X, Z, rank_rows, o_cols), buffer(X - 1, Z, rank_rows, o_cols),
            buffer(Z, rank_rows, o_cols), buffer(near_z, rank_rows, o_cols),
            buffer(Y, rank, q_cols), buffer(Y, rank, q_cols), pltpu.VMEM((Y, rank, q_cols), F32),
            buffer(X, *part_y), buffer(X - 1, *part_y), buffer(*part_y), buffer(Y - 1, *part_y[1:]),
            buffer(Y, *part_x), buffer(Y - 1, *part_x), buffer(*part_x), buffer(X - 1, *part_x[1:]),
            buffer(Z, rank_rows, q_cols), buffer(near_z, rank_rows, q_cols),
            dma(16), dma(15), dma(2, 4), dma(6),
            dma(Z - 1), dma(Z, X - 1), dma(Z), dma(Z - 1), dma(Z, X - 1), dma(Z),
            dma(Z - 1), dma(Z, X - 1), dma(Z - 1, Y - 1), dma(X - 1, Y - 1), dma(2),
            dma(X - 1), dma(Z), dma(Z), dma(Z - 1), dma(5),
            dma(Y), dma(2), dma(2, 2), dma(X - 1), dma(near_z), dma(Y), dma(X - 1), dma(Y - 1), dma(Y - 1), dma(X - 1), dma(near_z),
        ],
        compiler_params=pltpu.CompilerParams(collective_id=0, has_side_effects=True, vmem_limit_bytes=LIMIT),
        name="exchange",
    )(
        xin, qc, h, oc, qb, ob,
        qw, ow, qm, qs, om, os_,
    )
    qb_all, ob_all, wg_all, dg_all, qm_new, qs_new, om_new, os_new = outs
    (q_step, qw_new, q_copy, o_step, ow_new, o_copy, qm_new, qs_new, om_new, os_new) = pl.pallas_call(
        functools.partial(finish, X),
        out_shape=[
            shape(qw.shape, F32), shape(qw.shape, F32), shape((blocks * q_rows, q_cols), BF16),
            shape(ow.shape, F32), shape(ow.shape, F32), shape((blocks * o_rows, o_cols), BF16),
            shape(qm.shape, F32), shape(qs.shape, F32), shape(om.shape, F32), shape(os_.shape, F32),
        ],
        in_specs=[any_spec] * 4 + [vmem] * 6,
        out_specs=[vmem, vmem, any_spec, vmem, vmem, any_spec] + [vmem] * 4,
        scratch_shapes=[
            buffer(*qb_shape), buffer(*ob_shape), buffer(*wg_shape), buffer(*dg_shape),
            pltpu.VMEM((blocks * q_rows, q_cols), F32), pltpu.VMEM((blocks * o_rows, o_cols), F32),
            buffer(blocks * q_rows, q_cols), buffer(blocks * o_rows, o_cols),
            dma(6),
        ],
        compiler_params=pltpu.CompilerParams(vmem_limit_bytes=LIMIT),
        name="finish",
    )(qb_all, ob_all, wg_all, dg_all, qw, ow, qm_new, qs_new, om_new, os_new)
    return (qm_new, qs_new, q_step, qw_new, q_copy, om_new, os_new, o_step, ow_new, o_copy)


def solution(mesh, split=(8, 4, 4, 2)):
    cube = Mesh(mesh.devices.reshape(split), FS_TP)
    tokens = P(FS_TP, None)
    tile = P(FS, TP)
    return jax.shard_map(
        shards,
        mesh=cube,
        in_specs=(tokens,) * 4 + (tile, tile, P(FS, None), P(FS, None)) + (tile,) * 4,
        out_specs=(tile, tile, tile, tile, P(None, TP), tile, tile, tile, tile, P(None, TP)),
        check_vma=False,
    )
```

time: 74.7 us -> 72 us (0.964)
  Pallas kernels: 73 us -> 70.5 us
    pallas_call x1, Pallas kernels: 66.9 us -> 64.5 us  [shards(): pl.pallas_call(functools.partial(exchange, (Z, X, Y, token_scale)), out_s...]
where the time goes in v2:
time: 72 us; the launch traced here: 71.2 us
  Pallas kernels  70.5 us (98%)
    pallas_call x1, Pallas kernels, shards(): pl.pallas_call(functools.partial(exchange, (Z, X, Y, token_scale)), out_s...  64.5 us
    pallas_call x1, Pallas kernels, shards(): pl.pallas_call(functools.partial(finish, X), out_shape=[shape(qw.shape, F...  6.06 us

profile of v2, /device:TPU:8, one launch (start us, length us, event | category | flops | bytes accessed | tf_op | source)
XLA Modules:
  0.0 71.2 jit_solution(15415244094892166451)
XLA Ops:
  0.6 64.5 %exchange.1 = (bf16[8,4,2,64,256]{4,3,2,1,0:T(8,128)(2,1)}, bf16[8,4,2,32,256]{4,3,2,1,0:T(8,128)(2,1)}, bf16[8,4,128,128]{3,2,1,0:T(8,128)(2,1)}, bf16[8,4,16,3...) custom-call(bf16[768,2048]{1,0:T(8,128)(2,1)} %refs_0_.1, ...), custom_call_target="tpu_custom_call" | custom-call | tf_op jit(solution)/shard_map/exchange/pallas_call | solution.py:579
  65.1 6.1 %finish.1 = (f32[64,128]{1,0:T(8,128)}, f32[64,128]{1,0:T(8,128)}, bf16[2048,128]{1,0:T(8,128)(2,1)}, f32[32,256]{1,0:T(8,128)}, f32[32,256]{1,0:T(8,128)}, /*in...) custom-call(bf16[8,4,2,64,256]{4,3,2,1,0:T(8,128)(2,1)} %get-tuple-e, ...), custom_call_target="tpu_custom_call" | custom-call | tf_op jit(solution)/shard_map/finish/pallas_call | solution.py:614

commit v3 on v2

--- a/solution.py
+++ b/solution.py
@@ -28,11 +28,11 @@
 def exchange(sizes, *refs):
     Z, X, Y, token_scale = sizes
     (xin, qcin, hin, ocin, qbin, obin, qw_in, ow_in, qm_in, qs_in, om_in, os_in,
-     qb_out, ob_out, wg_out, dg_out, qm_out, qs_out, om_out, os_out,
-     QB, OB, WG, DG, vx, vqc, vh, voc, lot, lqt, qw, ow, qm, qs, om, os_,
+     qb_out, ob_out, wg_out, do_out, dq_out, qm_out, qs_out, om_out, os_out,
+     QB, OB, WG, DO, DQ, vx, vqc, vh, voc, lot, lqt, qw, ow, qm, qs, om, os_,
      pso, pro, mo, yso, ror, yro, xso, xro, zso, zro,
      psq, prq, mq, xsp, xrp, ysp, yrp, ysr, yrr, xsr, xrr, zsq, zrq,
-     loc, snd, a_send, b_send, rzo, rxo, pro_d, rzq, rxq, prq_d, rzb, rxb, ryb, rgb, pb, rxw, rrw, rlw, rzg, one,
+     loc, snd, a_send, rzo, rxo, pro_d, rzq, rxq, prq_d, rxw, rrw, rlw, rzg, rzh, d_send, one,
      s_pro, s_yrr, s_yro, s_xro, s_zro, s_prq, s_xrp, s_yrp, s_yrr2, s_xrr, s_zrq) = refs
     z, x, y, c = (lax.axis_index(name) for name in ("z", "x", "y", "c"))
     other = 1 - c
@@ -145,68 +145,6 @@
             sent(self.ref.at[0, pl.ds(0, X - 1), 0, self.rows], self.send.at[2])
             sent(self.ref.at[pl.ds(0, Z - 1), :, 0, self.rows], self.send.at[3])
 
-    class Shared:
-        def __init__(self, ref, first, send):
-            self.ref, self.first, self.send = ref, first, send
-            self.each = (ref.shape[3] - first) // Y
-
-        def rows(self, yy):
-            return pl.ds(pl.multiple_of(self.first + yy * self.each, 8), self.each)
-
-        def group(self, e, yy):
-            return self.ref.at[:, down(x, e, X), c, self.rows(yy)]
-
-        def along_z(self):
-            view = self.ref.at[z, x, c, self.rows(y)]
-            for d in zs:
-                to(view, view, self.send.at[0], rzb.at[d - 1], z=up(z, d, Z))
-
-        def along_x(self, d):
-            view = pieces(self.ref, d, 0, self.rows(y))
-            if d:
-                received(view, rzb.at[d - 1])
-            for e in xs:
-                to(view, view, self.send.at[1], rxb.at[d, e - 1], x=up(x, e, X))
-            if d:
-                for f in ys:
-                    to(view, view, self.send.at[2], ryb.at[d - 1, f - 1], y=up(y, f, Y))
-                to(view, view, self.send.at[4], pb.at[0], c=other)
-
-        def along_y(self):
-            for e in xs:
-                for d in [0] + zs:
-                    received(pieces(self.ref, d, e, self.rows(y)), rxb.at[d, e - 1])
-                view = self.group(e, y)
-                for f in ys:
-                    to(view, view, self.send.at[3], rgb.at[e - 1, f - 1], y=up(y, f, Y))
-                to(view, view, self.send.at[5], pb.at[1], c=other)
-
-        def arrive(self):
-            for d in zs:
-                for f in ys:
-                    view = pieces(self.ref, d, 0, self.rows(down(y, f, Y)))
-                    received(view, ryb.at[d - 1, f - 1])
-                    to(view, view, self.send.at[4], pb.at[0], c=other)
-            for e in xs:
-                for f in ys:
-                    view = self.group(e, down(y, f, Y))
-                    received(view, rgb.at[e - 1, f - 1])
-                    to(view, view, self.send.at[5], pb.at[1], c=other)
-
-        def region(self, grouped, times):
-            rows = pl.ds(self.first, times * self.each)
-            return self.ref.at[:, pl.ds(0, X - 1), 0, rows] if grouped else self.ref.at[pl.ds(0, Z - 1), 0, 0, rows]
-
-        def whole(self):
-            received(self.region(False, Y), pb.at[0])
-            received(self.region(True, Y), pb.at[1])
-
-        def done(self):
-            for number, (grouped, times) in enumerate(
-                ((False, 1), (True, 1), (False, Y - 1), (True, Y - 1), (False, Y), (True, Y))
-            ):
-                sent(self.region(grouped, times), self.send.at[number])
-
     class Weights:
         rights, lefts = Z // 2, Z - 1 - Z // 2
 
@@ -232,8 +170,7 @@
             sent(WG.at[pl.ds(0, Z - 1)], snd.at[1])
 
     gather_o = Gather(OB, o_rows, a_send.at[0], rzo, rxo, pro_d)
-    gather_q = Gather(QB, q_rows // 2, a_send.at[1], rzq, rxq, prq_d)
-    shared_q = Shared(QB, q_rows // 2, b_send)
+    gather_q = Gather(QB, q_rows, a_send.at[1], rzq, rxq, prq_d)
     weights = Weights()
     steps = list(range(1, weights.rights + 2))
 
@@ -246,13 +183,10 @@
     for number, d in enumerate(zs):
         gather_o.along_x(d)
         if number == min(1, len(zs) - 1):
-            shared_q.along_z()
             gather_q.along_z()
-    shared_q.along_x(0)
     gather_q.along_x(0)
-    for group in groups[1:-1]:
+    for group in groups[1:-2]:
         for d in group:
-            shared_q.along_x(d)
             gather_q.along_x(d)
     for group in groups:
         for d in group:
@@ -267,9 +201,9 @@
 
     get_h.wait()
     left(vh, OB, lot, c)
-    for d in groups[-1]:
-        shared_q.along_x(d)
-        gather_q.along_x(d)
+    for group in groups[max(1, len(groups) - 2) :]:
+        for d in group:
+            gather_q.along_x(d)
     gather_o.whole()
     put_ob = local(OB, ob_out, 14)
     left(vh, OB, lot, other)
@@ -343,10 +277,9 @@
         part_o(number, d)
         if number:
             pair_o(number - 1, order[number - 1])
-        if number == 0:
-            shared_q.along_y()
+        if number == 1:
             weights.along_x()
-        elif q_arrivals:
+        if number and q_arrivals:
             for e in q_arrivals.pop(0):
                 gather_q.arrive(e)
     pair_o(len(order) - 1, order[-1])
@@ -355,11 +288,11 @@
         for e in group:
             gather_q.arrive(e)
     weights_step()
-    shared_q.arrive()
+    for half in range(2):
+        ring_o.merge(half)
     get_x.wait()
     left(vx, QB, lqt, c)
     gather_q.whole()
-    shared_q.whole()
     put_qb = local(QB, qb_out, 15)
     left(vx, QB, lqt, other)
     get_qc.wait()
@@ -373,8 +306,6 @@
             psq[yy] = jnp.where(c == 0, high, low).astype(BF16)
             to(psq.at[yy], prq.at[yy], snd.at[4], s_prq.at[yy], c=other)
             mq[yy] = jnp.where(c == 0, low, high)
-    for half in range(2):
-        ring_o.merge(half)
     weights_step()
     low_rows = rank_rows // 2
     for d in ys + [0]:
@@ -445,23 +376,43 @@
     for d in zs:
         received(zro.at[d - 1], s_zro.at[d - 1])
         total = total + zro[d - 1].astype(F32)
-    DG[z, x, :, q_cols:] = moments(total * token_scale, om, os_)
+    DO[z, x] = moments(total * token_scale, om, os_)
+
+    class Directions:
+        def __init__(self, ref, send, rz, rx):
+            self.ref, self.send, self.rz, self.rx = ref, send, rz, rx
+
+        def along_z(self):
+            view = self.ref.at[z, x]
+            for d in zs:
+                to(view, view, self.send.at[0], self.rz.at[d - 1], z=up(z, d, Z))
+            self.along_x(0)
+
+        def along_x(self, d):
+            view = self.ref.at[down(z, d, Z), x]
+            if d:
+                received(view, self.rz.at[d - 1])
+            for e in xs:
+                to(view, view, self.send.at[1], self.rx, x=up(x, e, X))
+
+        def whole(self):
+            received(self.ref.at[:, pl.ds(0, X - 1)], self.rx)
+
+        def done(self):
+            sent(self.ref.at[pl.ds(0, Z - 1), 0], self.send.at[0])
+            sent(self.ref.at[:, pl.ds(0, X - 1)], self.send.at[1])
+
+    gather_do = Directions(DO, d_send.at[0], rzg, one.at[4])
+    gather_dq = Directions(DQ, d_send.at[1], rzh, one.at[3])
+    gather_do.along_z()
+
     total = zsq[z].astype(F32)
     for d in zs:
         received(zrq.at[d - 1], s_zrq.at[d - 1])
         total = total + zrq[d - 1].astype(F32)
-    DG[z, x, :, :q_cols] = moments(total * token_scale, qm, qs)
-
-    def direction_x(d):
-        view = DG.at[down(z, d, Z), x]
-        if d:
-            received(view, rzg.at[d - 1])
-        for e in xs:
-            to(view, view, snd.at[14], one.at[4], x=up(x, e, X))
-
-    for d in zs:
-        to(DG.at[z, x], DG.at[z, x], snd.at[10], rzg.at[d - 1], z=up(z, d, Z))
-    direction_x(0)
+    DQ[z, x] = moments(total * token_scale, qm, qs)
+
+    gather_dq.along_z()
     puts = [
         local(src, dst, number)
         for number, (src, dst) in enumerate(((qm, qm_out), (qs, qs_out), (om, om_out), (os_, os_out)))
@@ -469,12 +420,13 @@
     while steps:
         weights_step()
     for d in zs:
-        direction_x(d)
+        gather_do.along_x(d)
+    for d in zs:
+        gather_dq.along_x(d)
 
     put_wg = local(WG, wg_out, 4)
     gather_o.done()
     gather_q.done()
-    shared_q.done()
     weights.done()
     sent(pso, snd.at[2])
     ring_o.done()
@@ -490,67 +442,84 @@
     put_qb.wait()
     for copy in puts:
         copy.wait()
-    received(DG.at[:, pl.ds(0, X - 1)], one.at[4])
-    put_dg = local(DG, dg_out, 5)
-    sent(DG.at[pl.ds(0, Z - 1), 0], snd.at[10])
-    sent(DG.at[:, pl.ds(0, X - 1)], snd.at[14])
+    gather_do.whole()
+    put_do = local(DO, do_out, 5)
+    gather_dq.whole()
+    put_dq = local(DQ, dq_out, 6)
+    gather_do.done()
+    gather_dq.done()
     put_wg.wait()
-    put_dg.wait()
-
-
-def finish(X, qb_in, ob_in, wg_in, dg_in, qw, ow, qm, qs, om, os_, *refs):
+    put_do.wait()
+    put_dq.wait()
+
+
+def finish(X, qb_in, ob_in, wg_in, do_in, dq_in, qw_in, ow_in, qm_in, qs_in, om_in, os_in, *refs):
     (q_step, qw_new, q_copy, o_step, ow_new, o_copy, qm_out, qs_out, om_out, os_out,
-     QB, OB, WG, DG, qfull, ofull, vqc, voc, sem) = refs
+     QB, OB, WG, DO, DQ, qw, ow, qm, qs, om, os_, qstep, ostep, qfull, ofull, vqc, voc, sem) = refs
     fs = lax.axis_index("z") * X + lax.axis_index("x")
-    copies = []
-    for number, (src, dst) in enumerate(((dg_in, DG), (qb_in, QB), (ob_in, OB), (wg_in, WG))):
-        copies.append(pltpu.make_async_copy(src, dst, sem.at[number]))
-        copies[-1].start()
     q_cols, o_cols = qm.shape[1], om.shape[1]
     q_rows, o_rows = qw.shape[0], ow.shape[0]
     blocks = QB.shape[0] * QB.shape[1]
-    for src, dst in ((qm, qm_out), (qs, qs_out), (om, om_out), (os_, os_out)):
-        dst[...] = src[...]
-    copies[0].wait()
-    copies[1].wait()
     half_rank = QB.shape[4]
-
-    def product(B, columns):
-        directions = DG[:, :, :, columns].reshape(2 * half_rank, -1)
+    puts = []
+
+    def local(src, dst, number):
+        copy = pltpu.make_async_copy(src, dst, sem.at[number])
+        copy.start()
+        return copy
+
+    pairs = (
+        (dq_in, DQ), (qb_in, QB), (do_in, DO), (ob_in, OB), (wg_in, WG), (qw_in, qw), (ow_in, ow),
+        (qm_in, qm), (qs_in, qs), (om_in, om), (os_in, os_),
+    )
+    gets = [local(src, dst, number) for number, (src, dst) in enumerate(pairs)]
+
+    def product(B, D):
+        directions = D[...].reshape(2 * half_rank, -1)
         return sum(
             dot(B[:, :, half].reshape(-1, half_rank), directions[half * half_rank : (half + 1) * half_rank])
             for half in range(2)
         )
 
-    full = product(QB, slice(0, q_cols))
+    for number in (0, 1):
+        gets[number].wait()
+    full = product(QB, DQ)
     qfull[...] = full
-    q_scale = lax.rsqrt(jnp.sum(full * full, axis=0, keepdims=True) / (blocks * q_rows) + 0.05)
-    copies[2].wait()
-    full = product(OB, slice(q_cols, q_cols + o_cols))
+    scale = lax.rsqrt(jnp.sum(full * full, axis=0, keepdims=True) / (blocks * q_rows) + 0.05)
+    for number in (4, 5):
+        gets[number].wait()
+    vqc[...] = (
+        WG[:, :, 0:q_rows].reshape(blocks, q_rows, q_cols).astype(F32)
+        - 0.01 * (qfull[...] * scale).reshape(blocks, q_rows, q_cols)
+    ).astype(BF16).reshape(blocks * q_rows, q_cols)
+    puts.append(local(vqc, q_copy, 11))
+    step = qfull[pl.ds(pl.multiple_of(fs * q_rows, q_rows), q_rows), :] * scale
+    qstep[...] = step
+    qw[...] = qw[...] - 0.01 * step
+    puts.append(local(qstep, q_step, 12))
+    puts.append(local(qw, qw_new, 13))
+    for number in (2, 3, 6, 7, 8, 9, 10):
+        gets[number].wait()
+    for number, (src, dst) in enumerate(((qm, qm_out), (qs, qs_out), (om, om_out), (os_, os_out))):
+        puts.append(local(src, dst, 17 + number))
+    full = product(OB, DO)
     ofull[...] = full
-    o_scale = lax.rsqrt(jnp.sum(full * full, axis=0, keepdims=True) / (blocks * o_rows) + 0.05)
-    copies[3].wait()
-    vqc[...] = (
-        WG[:, :, 0:q_rows].reshape(blocks, q_rows, q_cols).astype(F32) - 0.01 * (qfull[...] * q_scale).reshape(blocks, q_rows, q_cols)
-    ).astype(BF16).reshape(blocks * q_rows, q_cols)
-    put_q = pltpu.make_async_copy(vqc, q_copy, sem.at[4])
-    put_q.start()
+    scale = lax.rsqrt(jnp.sum(full * full, axis=0, keepdims=True) / (blocks * o_rows) + 0.05)
     for half in range(o_cols // q_cols):
         part = slice(half * q_cols, (half + 1) * q_cols)
         rows = slice(q_rows + half * o_rows, q_rows + (half + 1) * o_rows)
         voc[:, part] = (
-            WG[:, :, rows].reshape(blocks, o_rows, q_cols).astype(F32) - 0.01 * (ofull[:, part] * o_scale[:, part]).reshape(blocks, o_rows, q_cols)
+            WG[:, :, rows].reshape(blocks, o_rows, q_cols).astype(F32)
+            - 0.01 * (ofull[:, part] * scale[:, part]).reshape(blocks, o_rows, q_cols)
         ).astype(BF16).reshape(blocks * o_rows, q_cols)
-    put_o = pltpu.make_async_copy(voc, o_copy, sem.at[5])
-    put_o.start()
-    step = qfull[pl.ds(pl.multiple_of(fs * q_rows, q_rows), q_rows), :] * q_scale
-    q_step[...] = step
-    qw_new[...] = qw[...] - 0.01 * step
-    step = ofull[pl.ds(pl.multiple_of(fs * o_rows, o_rows), o_rows), :] * o_scale
-    o_step[...] = step
-    ow_new[...] = ow[...] - 0.01 * step
-    put_q.wait()
-    put_o.wait()
+    puts.append(local(voc, o_copy, 14))
+    step = ofull[pl.ds(pl.multiple_of(fs * o_rows, o_rows), o_rows), :] * scale
+    ostep[...] = step
+    ow[...] = ow[...] - 0.01 * step
+    puts.append(local(ostep, o_step, 15))
+    puts.append(local(ow, ow_new, 16))
+    for copy in puts:
+        copy.wait()
 
 
 def shards(xin, qc, h, oc, qw, ow, qb, ob, qm, qs, om, os_):
@@ -565,12 +534,12 @@
     halves = o_cols // q_cols
     w_rows = q_rows + halves * o_rows
     any_spec = pl.BlockSpec(memory_space=pl.ANY)
-    vmem = pl.BlockSpec(memory_space=pltpu.VMEM)
     shape = jax.ShapeDtypeStruct
     qb_shape = (Z, X, 2, q_rows, rank // 2)
     ob_shape = (Z, X, 2, o_rows, rank // 2)
     wg_shape = (Z, X, w_rows, q_cols)
-    dg_shape = (Z, X, rank_rows, q_cols + o_cols)
+    do_shape = (Z, X, rank_rows, o_cols)
+    dq_shape = (Z, X, rank_rows, q_cols)
     near_z = max(Z - 1, 1)
     part_x = (X, Z, rank_rows // 2, q_cols)
     part_y = (Y, Z, rank_rows // 2, q_cols)
@@ -579,13 +548,14 @@
     outs = pl.pallas_call(
         functools.partial(exchange, (Z, X, Y, token_scale)),
         out_shape=[
-            shape(qb_shape, BF16), shape(ob_shape, BF16), shape(wg_shape, BF16), shape(dg_shape, BF16),
+            shape(qb_shape, BF16), shape(ob_shape, BF16), shape(wg_shape, BF16), shape(do_shape, BF16),
+            shape(dq_shape, BF16),
             shape(qm.shape, F32), shape(qs.shape, F32), shape(om.shape, F32), shape(os_.shape, F32),
         ],
         in_specs=[any_spec] * 12,
-        out_specs=[any_spec] * 8,
+        out_specs=[any_spec] * 9,
         scratch_shapes=[
-            buffer(*qb_shape), buffer(*ob_shape), buffer(*wg_shape), buffer(*dg_shape),
+            buffer(*qb_shape), buffer(*ob_shape), buffer(*wg_shape), buffer(*do_shape), buffer(*dq_shape),
             buffer(tokens, model), buffer(tokens, wide), buffer(tokens, wide), buffer(tokens, model),
             buffer(2, rank // 2, tokens), buffer(2, rank // 2, tokens),
             pltpu.VMEM(qw.shape, F32), pltpu.VMEM(ow.shape, F32), pltpu.VMEM(qm.shape, F32),
@@ -598,10 +568,9 @@
             buffer(X, *part_y), buffer(X - 1, *part_y), buffer(*part_y), buffer(Y - 1, *part_y[1:]),
             buffer(Y, *part_x), buffer(Y - 1, *part_x), buffer(*part_x), buffer(X - 1, *part_x[1:]),
             buffer(Z, rank_rows, q_cols), buffer(near_z, rank_rows, q_cols),
-            dma(16), dma(15), dma(2, 4), dma(6),
+            dma(16), dma(15), dma(2, 4),
             dma(Z - 1), dma(Z, X - 1), dma(Z), dma(Z - 1), dma(Z, X - 1), dma(Z),
-            dma(Z - 1), dma(Z, X - 1), dma(Z - 1, Y - 1), dma(X - 1, Y - 1), dma(2),
-            dma(X - 1), dma(Z), dma(Z), dma(Z - 1), dma(5),
+            dma(X - 1), dma(Z), dma(Z), dma(Z - 1), dma(Z - 1), dma(2, 2), dma(5),
             dma(Y), dma(2), dma(2, 2), dma(X - 1), dma(near_z), dma(Y), dma(X - 1), dma(Y - 1), dma(Y - 1), dma(X - 1), dma(near_z),
         ],
         compiler_params=pltpu.CompilerParams(collective_id=0, has_side_effects=True, vmem_limit_bytes=LIMIT),
@@ -610,7 +579,7 @@
         xin, qc, h, oc, qb, ob,
         qw, ow, qm, qs, om, os_,
     )
-    qb_all, ob_all, wg_all, dg_all, qm_new, qs_new, om_new, os_new = outs
+    qb_all, ob_all, wg_all, do_all, dq_all, qm_new, qs_new, om_new, os_new = outs
     (q_step, qw_new, q_copy, o_step, ow_new, o_copy, qm_new, qs_new, om_new, os_new) = pl.pallas_call(
         functools.partial(finish, X),
         out_shape=[
@@ -618,17 +587,20 @@
             shape(ow.shape, F32), shape(ow.shape, F32), shape((blocks * o_rows, o_cols), BF16),
             shape(qm.shape, F32), shape(qs.shape, F32), shape(om.shape, F32), shape(os_.shape, F32),
         ],
-        in_specs=[any_spec] * 4 + [vmem] * 6,
-        out_specs=[vmem, vmem, any_spec, vmem, vmem, any_spec] + [vmem] * 4,
+        in_specs=[any_spec] * 11,
+        out_specs=[any_spec] * 10,
         scratch_shapes=[
-            buffer(*qb_shape), buffer(*ob_shape), buffer(*wg_shape), buffer(*dg_shape),
+            buffer(*qb_shape), buffer(*ob_shape), buffer(*wg_shape), buffer(*do_shape), buffer(*dq_shape),
+            pltpu.VMEM(qw.shape, F32), pltpu.VMEM(ow.shape, F32), pltpu.VMEM(qm.shape, F32),
+            pltpu.VMEM(qs.shape, F32), pltpu.VMEM(om.shape, F32), pltpu.VMEM(os_.shape, F32),
+            pltpu.VMEM(qw.shape, F32), pltpu.VMEM(ow.shape, F32),
             pltpu.VMEM((blocks * q_rows, q_cols), F32), pltpu.VMEM((blocks * o_rows, o_cols), F32),
             buffer(blocks * q_rows, q_cols), buffer(blocks * o_rows, o_cols),
-            dma(6),
+            dma(21),
         ],
         compiler_params=pltpu.CompilerParams(vmem_limit_bytes=LIMIT),
         name="finish",
-    )(qb_all, ob_all, wg_all, dg_all, qw, ow, qm_new, qs_new, om_new, os_new)
+    )(qb_all, ob_all, wg_all, do_all, dq_all, qw, ow, qm_new, qs_new, om_new, os_new)
     return (qm_new, qs_new, q_step, qw_new, q_copy, om_new, os_new, o_step, ow_new, o_copy)
 
 

time: 72 us -> 67.1 us (0.932)
  Pallas kernels: 70.5 us -> 65.9 us
    pallas_call x1, Pallas kernels: 64.5 us -> 61.2 us  [shards(): pl.pallas_call(functools.partial(exchange, (Z, X, Y, token_scale)), out_s...]
    pallas_call x1, Pallas kernels: 6.06 us -> 4.78 us  [shards(): pl.pallas_call(functools.partial(finish, X), out_shape=[shape(qw.shape, F...]
where the time goes in v3:
time: 67.1 us; the launch traced here: 66.6 us
  Pallas kernels  65.9 us (98%)
    pallas_call x1, Pallas kernels, shards(): pl.pallas_call(functools.partial(exchange, (Z, X, Y, token_scale)), out_s...  61.2 us
    pallas_call x1, Pallas kernels, shards(): pl.pallas_call(functools.partial(finish, X), out_shape=[shape(qw.shape, F...  4.78 us

profile of v3, /device:TPU:8, one launch (start us, length us, event | category | flops | bytes accessed | tf_op | source)
XLA Modules:
  0.0 66.6 jit_solution(2757124567328621630)
XLA Ops:
  0.6 61.2 %exchange.1 = (bf16[8,4,2,64,256]{4,3,2,1,0:T(8,128)(2,1)}, bf16[8,4,2,32,256]{4,3,2,1,0:T(8,128)(2,1)}, bf16[8,4,128,128]{3,2,1,0:T(8,128)(2,1)}, bf16[8,4,16,2...) custom-call(bf16[768,2048]{1,0:T(8,128)(2,1)} %refs_0_.1, ...), custom_call_target="tpu_custom_call" | custom-call | tf_op jit(solution)/shard_map/exchange/pallas_call | solution.py:548
  61.8 4.8 %finish.1 = (f32[64,128]{1,0:T(8,128)}, f32[64,128]{1,0:T(8,128)}, bf16[2048,128]{1,0:T(8,128)(2,1)}, f32[32,256]{1,0:T(8,128)}, f32[32,256]{1,0:T(8,128)}, /*in...) custom-call(bf16[8,4,2,64,256]{4,3,2,1,0:T(8,128)(2,1)} %get-tuple-e, ...), custom_call_target="tpu_custom_call" | custom-call | tf_op jit(solution)/shard_map/finish/pallas_call | solution.py:583

commit v4 on v3

--- a/solution.py
+++ b/solution.py
@@ -14,7 +14,7 @@
 MESH = pl.DeviceIdType.MESH
 F32 = jnp.float32
 BF16 = jnp.bfloat16
-LIMIT = 60 * 1024 * 1024
+LIMIT = 62_300_000
 
 
 def nearest_first(n):
@@ -28,8 +28,8 @@
 def exchange(sizes, *refs):
     Z, X, Y, token_scale = sizes
     (xin, qcin, hin, ocin, qbin, obin, qw_in, ow_in, qm_in, qs_in, om_in, os_in,
-     qb_out, ob_out, wg_out, do_out, dq_out, qm_out, qs_out, om_out, os_out,
-     QB, OB, WG, DO, DQ, vx, vqc, vh, voc, lot, lqt, qw, ow, qm, qs, om, os_,
+     QB, OB, WG, DO, DQ, qm, qs, om, os_,
+     vx, vqc, vh, voc, lot, lqt, qw, ow,
      pso, pro, mo, yso, ror, yro, xso, xro, zso, zro,
      psq, prq, mq, xsp, xrp, ysp, yrp, ysr, yrr, xsr, xrr, zsq, zrq,
      loc, snd, a_send, rzo, rxo, pro_d, rzq, rxq, prq_d, rxw, rrw, rlw, rzg, rzh, d_send, one,
@@ -205,7 +205,6 @@
         for d in group:
             gather_q.along_x(d)
     gather_o.whole()
-    put_ob = local(OB, ob_out, 14)
     left(vh, OB, lot, other)
     get_oc.wait()
     q_arrivals = list(groups)
@@ -293,7 +292,6 @@
     get_x.wait()
     left(vx, QB, lqt, c)
     gather_q.whole()
-    put_qb = local(QB, qb_out, 15)
     left(vx, QB, lqt, other)
     get_qc.wait()
     each = Y // 2
@@ -413,10 +411,6 @@
     DQ[z, x] = moments(total * token_scale, qm, qs)
 
     gather_dq.along_z()
-    puts = [
-        local(src, dst, number)
-        for number, (src, dst) in enumerate(((qm, qm_out), (qs, qs_out), (om, om_out), (os_, os_out)))
-    ]
     while steps:
         weights_step()
     for d in zs:
@@ -424,7 +418,6 @@
     for d in zs:
         gather_dq.along_x(d)
 
-    put_wg = local(WG, wg_out, 4)
     gather_o.done()
     gather_q.done()
     weights.done()
@@ -438,24 +431,15 @@
     sent(zrq, snd.at[7])
     sent(zro, snd.at[8])
     sent(yrp, snd.at[11])
-    put_ob.wait()
-    put_qb.wait()
-    for copy in puts:
-        copy.wait()
     gather_do.whole()
-    put_do = local(DO, do_out, 5)
     gather_dq.whole()
-    put_dq = local(DQ, dq_out, 6)
     gather_do.done()
     gather_dq.done()
-    put_wg.wait()
-    put_do.wait()
-    put_dq.wait()
-
-
-def finish(X, qb_in, ob_in, wg_in, do_in, dq_in, qw_in, ow_in, qm_in, qs_in, om_in, os_in, *refs):
+
+
+def finish(X, QB, OB, WG, DO, DQ, qw, ow, qm, qs, om, os_, *refs):
     (q_step, qw_new, q_copy, o_step, ow_new, o_copy, qm_out, qs_out, om_out, os_out,
-     QB, OB, WG, DO, DQ, qw, ow, qm, qs, om, os_, qstep, ostep, qfull, ofull, vqc, voc, sem) = refs
+     qstep, ostep, qnew, onew, qfull, ofull, vqc, voc, sem) = refs
     fs = lax.axis_index("z") * X + lax.axis_index("x")
     q_cols, o_cols = qm.shape[1], om.shape[1]
     q_rows, o_rows = qw.shape[0], ow.shape[0]
@@ -468,11 +452,8 @@
         copy.start()
         return copy
 
-    pairs = (
-        (dq_in, DQ), (qb_in, QB), (do_in, DO), (ob_in, OB), (wg_in, WG), (qw_in, qw), (ow_in, ow),
-        (qm_in, qm), (qs_in, qs), (om_in, om), (os_in, os_),
-    )
-    gets = [local(src, dst, number) for number, (src, dst) in enumerate(pairs)]
+    for number, (src, dst) in enumerate(((qm, qm_out), (qs, qs_out), (om, om_out), (os_, os_out))):
+        puts.append(local(src, dst, 6 + number))
 
     def product(B, D):
         directions = D[...].reshape(2 * half_rank, -1)
@@ -481,27 +462,19 @@
             for half in range(2)
         )
 
-    for number in (0, 1):
-        gets[number].wait()
     full = product(QB, DQ)
     qfull[...] = full
     scale = lax.rsqrt(jnp.sum(full * full, axis=0, keepdims=True) / (blocks * q_rows) + 0.05)
-    for number in (4, 5):
-        gets[number].wait()
     vqc[...] = (
         WG[:, :, 0:q_rows].reshape(blocks, q_rows, q_cols).astype(F32)
         - 0.01 * (qfull[...] * scale).reshape(blocks, q_rows, q_cols)
     ).astype(BF16).reshape(blocks * q_rows, q_cols)
-    puts.append(local(vqc, q_copy, 11))
+    puts.append(local(vqc, q_copy, 0))
     step = qfull[pl.ds(pl.multiple_of(fs * q_rows, q_rows), q_rows), :] * scale
     qstep[...] = step
-    qw[...] = qw[...] - 0.01 * step
-    puts.append(local(qstep, q_step, 12))
-    puts.append(local(qw, qw_new, 13))
-    for number in (2, 3, 6, 7, 8, 9, 10):
-        gets[number].wait()
-    for number, (src, dst) in enumerate(((qm, qm_out), (qs, qs_out), (om, om_out), (os_, os_out))):
-        puts.append(local(src, dst, 17 + number))
+    qnew[...] = qw[...] - 0.01 * step
+    puts.append(local(qstep, q_step, 1))
+    puts.append(local(qnew, qw_new, 2))
     full = product(OB, DO)
     ofull[...] = full
     scale = lax.rsqrt(jnp.sum(full * full, axis=0, keepdims=True) / (blocks * o_rows) + 0.05)
@@ -512,12 +485,12 @@
             WG[:, :, rows].reshape(blocks, o_rows, q_cols).astype(F32)
             - 0.01 * (ofull[:, part] * scale[:, part]).reshape(blocks, o_rows, q_cols)
         ).astype(BF16).reshape(blocks * o_rows, q_cols)
-    puts.append(local(voc, o_copy, 14))
+    puts.append(local(voc, o_copy, 3))
     step = ofull[pl.ds(pl.multiple_of(fs * o_rows, o_rows), o_rows), :] * scale
     ostep[...] = step
-    ow[...] = ow[...] - 0.01 * step
-    puts.append(local(ostep, o_step, 15))
-    puts.append(local(ow, ow_new, 16))
+    onew[...] = ow[...] - 0.01 * step
+    puts.append(local(ostep, o_step, 4))
+    puts.append(local(onew, ow_new, 5))
     for copy in puts:
         copy.wait()
 
@@ -533,7 +506,8 @@
     token_scale = (tokens * blocks * Y * C) ** (-0.5)
     halves = o_cols // q_cols
     w_rows = q_rows + halves * o_rows
-    any_spec = pl.BlockSpec(memory_space=pl.ANY)
+    vmem = pl.BlockSpec(memory_space=pltpu.VMEM)
+    any_spec = pl.BlockSpec(memory_space=pltpu.HBM)
     shape = jax.ShapeDtypeStruct
     qb_shape = (Z, X, 2, q_rows, rank // 2)
     ob_shape = (Z, X, 2, o_rows, rank // 2)
@@ -548,18 +522,16 @@
     outs = pl.pallas_call(
         functools.partial(exchange, (Z, X, Y, token_scale)),
         out_shape=[
-            shape(qb_shape, BF16), shape(ob_shape, BF16), shape(wg_shape, BF16), shape(do_shape, BF16),
-            shape(dq_shape, BF16),
-            shape(qm.shape, F32), shape(qs.shape, F32), shape(om.shape, F32), shape(os_.shape, F32),
+            pltpu.VMEM(qb_shape, BF16), pltpu.VMEM(ob_shape, BF16), pltpu.VMEM(wg_shape, BF16), pltpu.VMEM(do_shape, BF16),
+            pltpu.VMEM(dq_shape, BF16),
+            pltpu.VMEM(qm.shape, F32), pltpu.VMEM(qs.shape, F32), pltpu.VMEM(om.shape, F32), pltpu.VMEM(os_.shape, F32),
         ],
         in_specs=[any_spec] * 12,
-        out_specs=[any_spec] * 9,
+        out_specs=[vmem] * 9,
         scratch_shapes=[
-            buffer(*qb_shape), buffer(*ob_shape), buffer(*wg_shape), buffer(*do_shape), buffer(*dq_shape),
             buffer(tokens, model), buffer(tokens, wide), buffer(tokens, wide), buffer(tokens, model),
             buffer(2, rank // 2, tokens), buffer(2, rank // 2, tokens),
-            pltpu.VMEM(qw.shape, F32), pltpu.VMEM(ow.shape, F32), pltpu.VMEM(qm.shape, F32),
-            pltpu.VMEM(qs.shape, F32), pltpu.VMEM(om.shape, F32), pltpu.VMEM(os_.shape, F32),
+            pltpu.VMEM(qw.shape, F32), pltpu.VMEM(ow.shape, F32),
             buffer(Y, rank, o_cols), buffer(Y, rank, o_cols), pltpu.VMEM((2, rank, o_cols), F32),
             buffer(Y, 2, rank // 2, o_cols), buffer(2, rank // 2, o_cols), buffer(2, 2, rank // 2, o_cols),
             buffer(X, Z, rank_rows, o_cols), buffer(X - 1, Z, rank_rows, o_cols),
@@ -587,18 +559,15 @@
             shape(ow.shape, F32), shape(ow.shape, F32), shape((blocks * o_rows, o_cols), BF16),
             shape(qm.shape, F32), shape(qs.shape, F32), shape(om.shape, F32), shape(os_.shape, F32),
         ],
-        in_specs=[any_spec] * 11,
+        in_specs=[vmem] * 11,
         out_specs=[any_spec] * 10,
         scratch_shapes=[
-            buffer(*qb_shape), buffer(*ob_shape), buffer(*wg_shape), buffer(*do_shape), buffer(*dq_shape),
-            pltpu.VMEM(qw.shape, F32), pltpu.VMEM(ow.shape, F32), pltpu.VMEM(qm.shape, F32),
-            pltpu.VMEM(qs.shape, F32), pltpu.VMEM(om.shape, F32), pltpu.VMEM(os_.shape, F32),
-            pltpu.VMEM(qw.shape, F32), pltpu.VMEM(ow.shape, F32),
+            pltpu.VMEM(qw.shape, F32), pltpu.VMEM(ow.shape, F32), pltpu.VMEM(qw.shape, F32), pltpu.VMEM(ow.shape, F32),
             pltpu.VMEM((blocks * q_rows, q_cols), F32), pltpu.VMEM((blocks * o_rows, o_cols), F32),
             buffer(blocks * q_rows, q_cols), buffer(blocks * o_rows, o_cols),
-            dma(21),
+            dma(10),
         ],
-        compiler_params=pltpu.CompilerParams(vmem_limit_bytes=LIMIT),
+        compiler_params=pltpu.CompilerParams(vmem_limit_bytes=LIMIT // 2),
         name="finish",
     )(qb_all, ob_all, wg_all, do_all, dq_all, qw, ow, qm_new, qs_new, om_new, os_new)
     return (qm_new, qs_new, q_step, qw_new, q_copy, om_new, os_new, o_step, ow_new, o_copy)

time: 67.1 us -> 64.2 us (0.957)
  Pallas kernels: 65.9 us -> 62.9 us
    pallas_call x1, Pallas kernels: 4.78 us -> 2.46 us  [shards(): pl.pallas_call(functools.partial(finish, X), out_shape=[shape(qw.shape, F...]
    pallas_call x1, Pallas kernels: 61.2 us -> 60.5 us  [shards(): pl.pallas_call(functools.partial(exchange, (Z, X, Y, token_scale)), out_s...]
where the time goes in v4:
time: 64.2 us; the launch traced here: 63.6 us
  Pallas kernels  62.9 us (98%)
  between operations  0.69 us (1%)
    pallas_call x1, Pallas kernels, shards(): pl.pallas_call(functools.partial(exchange, (Z, X, Y, token_scale)), out_s...  60.5 us
    pallas_call x1, Pallas kernels, shards(): pl.pallas_call(functools.partial(finish, X), out_shape=[shape(qw.shape, F...  2.46 us

profile of v4, /device:TPU:8, one launch (start us, length us, event | category | flops | bytes accessed | tf_op | source)
XLA Modules:
  0.0 63.6 jit_solution(13322508698408316741)
XLA Ops:
  0.6 0.0 copy-start.1
  0.7 0.0 copy-start
  0.7 60.5 %exchange.1 = (bf16[8,4,2,64,256]{4,3,2,1,0:T(8,128)(2,1)S(1)}, bf16[8,4,2,32,256]{4,3,2,1,0:T(8,128)(2,1)S(1)}, bf16[8,4,128,128]{3,2,1,0:T(8,128)(2,1)S(1)}, b...) custom-call(bf16[768,2048]{1,0:T(8,128)(2,1)} %refs_0_.1, ...), custom_call_target="tpu_custom_call" | custom-call | tf_op jit(solution)/shard_map/exchange/pallas_call | solution.py:522
  61.1 0.0 copy-done.1
  61.1 0.0 copy-done
  61.1 2.5 %finish.1 = (f32[64,128]{1,0:T(8,128)}, f32[64,128]{1,0:T(8,128)}, bf16[2048,128]{1,0:T(8,128)(2,1)}, f32[32,256]{1,0:T(8,128)}, f32[32,256]{1,0:T(8,128)}, /*in...) custom-call(bf16[8,4,2,64,256]{4,3,2,1,0:T(8,128)(2,1)S(1)} %get-tup, ...), custom_call_target="tpu_custom_call" | custom-call | tf_op jit(solution)/shard_map/finish/pallas_call | solution.py:555
Async XLA Ops:
  0.6 60.5 %copy-start.1 = (f32[32,256]{1,0:T(8,128)S(1)}, f32[32,256]{1,0:T(8,128)}, u32[]{:S(2)}) copy-start(f32[32,256]{1,0:T(8,128)} %ow.1) | copy-start | bytes 98308
  0.7 60.5 %copy-start = (f32[64,128]{1,0:T(8,128)S(1)}, f32[64,128]{1,0:T(8,128)}, u32[]{:S(2)}) copy-start(f32[64,128]{1,0:T(8,128)} %qw.1) | copy-start | bytes 98308

commit v5 on v4

--- a/solution.py
+++ b/solution.py
@@ -180,6 +180,7 @@
 
     gather_o.along_z()
     gather_o.along_x(0)
+    weights.along_x()
     for number, d in enumerate(zs):
         gather_o.along_x(d)
         if number == min(1, len(zs) - 1):
@@ -206,6 +207,7 @@
             gather_q.along_x(d)
     gather_o.whole()
     left(vh, OB, lot, other)
+    weights_step()
     get_oc.wait()
     q_arrivals = list(groups)
 
@@ -276,8 +278,6 @@
         part_o(number, d)
         if number:
             pair_o(number - 1, order[number - 1])
-        if number == 1:
-            weights.along_x()
         if number and q_arrivals:
             for e in q_arrivals.pop(0):
                 gather_q.arrive(e)
@@ -361,7 +361,6 @@
     for d in zs:
         zz = up(z, d, Z)
         to(zsq.at[zz], zrq.at[d - 1], snd.at[7], s_zrq.at[d - 1], z=zz)
-    weights_step()
 
     def moments(reduced, mean, square):
         mean_new = 0.8 * mean[...] + 0.2 * reduced

time: 64.2 us -> 62.4 us (0.972)
  Pallas kernels: 62.9 us -> 61.6 us
    pallas_call x1, Pallas kernels: 60.5 us -> 59.2 us  [shards(): pl.pallas_call(functools.partial(exchange, (Z, X, Y, token_scale)), out_s...]
where the time goes in v5:
time: 62.4 us; the launch traced here: 62.3 us
  Pallas kernels  61.6 us (99%)
  between operations  0.69 us (1%)
    pallas_call x1, Pallas kernels, shards(): pl.pallas_call(functools.partial(exchange, (Z, X, Y, token_scale)), out_s...  59.2 us
    pallas_call x1, Pallas kernels, shards(): pl.pallas_call(functools.partial(finish, X), out_shape=[shape(qw.shape, F...  2.47 us

profile of v5, /device:TPU:8, one launch (start us, length us, event | category | flops | bytes accessed | tf_op | source)
XLA Modules:
  0.0 62.3 jit_solution(6994166401287089342)
XLA Ops:
  0.6 0.0 copy-start.1
  0.7 0.0 copy-start
  0.7 59.2 %exchange.1 = (bf16[8,4,2,64,256]{4,3,2,1,0:T(8,128)(2,1)S(1)}, bf16[8,4,2,32,256]{4,3,2,1,0:T(8,128)(2,1)S(1)}, bf16[8,4,128,128]{3,2,1,0:T(8,128)(2,1)S(1)}, b...) custom-call(bf16[768,2048]{1,0:T(8,128)(2,1)} %refs_0_.1, ...), custom_call_target="tpu_custom_call" | custom-call | tf_op jit(solution)/shard_map/exchange/pallas_call | solution.py:521
  59.8 0.0 copy-done.1
  59.9 0.0 copy-done
  59.9 2.5 %finish.1 = (f32[64,128]{1,0:T(8,128)}, f32[64,128]{1,0:T(8,128)}, bf16[2048,128]{1,0:T(8,128)(2,1)}, f32[32,256]{1,0:T(8,128)}, f32[32,256]{1,0:T(8,128)}, /*in...) custom-call(bf16[8,4,2,64,256]{4,3,2,1,0:T(8,128)(2,1)S(1)} %get-tup, ...), custom_call_target="tpu_custom_call" | custom-call | tf_op jit(solution)/shard_map/finish/pallas_call | solution.py:554
Async XLA Ops:
  0.6 59.2 %copy-start.1 = (f32[32,256]{1,0:T(8,128)S(1)}, f32[32,256]{1,0:T(8,128)}, u32[]{:S(2)}) copy-start(f32[32,256]{1,0:T(8,128)} %ow.1) | copy-start | bytes 98308
  0.7 59.2 %copy-start = (f32[64,128]{1,0:T(8,128)S(1)}, f32[64,128]{1,0:T(8,128)}, u32[]{:S(2)}) copy-start(f32[64,128]{1,0:T(8,128)} %qw.1) | copy-start | bytes 98308

commit v6 on v5

--- a/solution.py
+++ b/solution.py
@@ -29,7 +29,7 @@
     Z, X, Y, token_scale = sizes
     (xin, qcin, hin, ocin, qbin, obin, qw_in, ow_in, qm_in, qs_in, om_in, os_in,
      QB, OB, WG, DO, DQ, qm, qs, om, os_,
-     vx, vqc, vh, voc, lot, lqt, qw, ow,
+     vx, vqc, vh, voc, lot, lqt, qw, ow, acc,
      pso, pro, mo, yso, ror, yro, xso, xro, zso, zro,
      psq, prq, mq, xsp, xrp, ysp, yrp, ysr, yrr, xsr, xrr, zsq, zrq,
      loc, snd, a_send, rzo, rxo, pro_d, rzq, rxq, prq_d, rxw, rrw, rlw, rzg, rzh, d_send, one,
@@ -283,14 +283,33 @@
                 gather_q.arrive(e)
     pair_o(len(order) - 1, order[-1])
 
+    get_x.wait()
+    place = X * q_rows
+
+    def left_part(ds):
+        for part in range(2):
+            count = vx.shape[0] // 2
+            at = slice(part * count, (part + 1) * count)
+            total = None
+            for d in ds:
+                zz = down(z, d, Z)
+                columns = pl.ds(pl.multiple_of(zz * place, place), place)
+                term = dot(vx[at, columns], QB[zz, :, c].reshape(place, half_rank))
+                total = term if total is None else total + term
+            yield at, total
+
+    here = [d for group in groups[: max(1, len(groups) - 2)] for d in group]
+    rest = [d for group in groups[max(1, len(groups) - 2) :] for d in group]
+    for at, total in left_part(here):
+        acc[at] = total
     for group in q_arrivals:
         for e in group:
             gather_q.arrive(e)
     weights_step()
     for half in range(2):
         ring_o.merge(half)
-    get_x.wait()
-    left(vx, QB, lqt, c)
+    for at, total in left_part(rest):
+        lqt[c, :, at] = (acc[at] + total).astype(BF16).T
     gather_q.whole()
     left(vx, QB, lqt, other)
     get_qc.wait()
@@ -530,7 +549,7 @@
         scratch_shapes=[
             buffer(tokens, model), buffer(tokens, wide), buffer(tokens, wide), buffer(tokens, model),
             buffer(2, rank // 2, tokens), buffer(2, rank // 2, tokens),
-            pltpu.VMEM(qw.shape, F32), pltpu.VMEM(ow.shape, F32),
+            pltpu.VMEM(qw.shape, F32), pltpu.VMEM(ow.shape, F32), pltpu.VMEM((tokens, rank // 2), F32),
             buffer(Y, rank, o_cols), buffer(Y, rank, o_cols), pltpu.VMEM((2, rank, o_cols), F32),
             buffer(Y, 2, rank // 2, o_cols), buffer(2, rank // 2, o_cols), buffer(2, 2, rank // 2, o_cols),
             buffer(X, Z, rank_rows, o_cols), buffer(X - 1, Z, rank_rows, o_cols),

time: 62.4 us -> 62.4 us (level)
  no operation moved by 1% of the time
where the time goes in v6:
time: 62.4 us; the launch traced here: 62 us
  Pallas kernels  61.3 us (98%)
  between operations  0.69 us (1%)
    pallas_call x1, Pallas kernels, shards(): pl.pallas_call(functools.partial(exchange, (Z, X, Y, token_scale)), out_s...  58.9 us
    pallas_call x1, Pallas kernels, shards(): pl.pallas_call(functools.partial(finish, X), out_shape=[shape(qw.shape, F...  2.47 us

profile of v6, /device:TPU:8, one launch (start us, length us, event | category | flops | bytes accessed | tf_op | source)
XLA Modules:
  0.0 62.0 jit_solution(21870578915051427)
XLA Ops:
  0.6 0.0 copy-start.1
  0.7 0.0 copy-start
  0.7 58.9 %exchange.1 = (bf16[8,4,2,64,256]{4,3,2,1,0:T(8,128)(2,1)S(1)}, bf16[8,4,2,32,256]{4,3,2,1,0:T(8,128)(2,1)S(1)}, bf16[8,4,128,128]{3,2,1,0:T(8,128)(2,1)S(1)}, b...) custom-call(bf16[768,2048]{1,0:T(8,128)(2,1)} %refs_0_.1, ...), custom_call_target="tpu_custom_call" | custom-call | tf_op jit(solution)/shard_map/exchange/pallas_call | solution.py:540
  59.5 0.0 copy-done.1
  59.6 0.0 copy-done
  59.6 2.5 %finish.1 = (f32[64,128]{1,0:T(8,128)}, f32[64,128]{1,0:T(8,128)}, bf16[2048,128]{1,0:T(8,128)(2,1)}, f32[32,256]{1,0:T(8,128)}, f32[32,256]{1,0:T(8,128)}, /*in...) custom-call(bf16[8,4,2,64,256]{4,3,2,1,0:T(8,128)(2,1)S(1)} %get-tup, ...), custom_call_target="tpu_custom_call" | custom-call | tf_op jit(solution)/shard_map/finish/pallas_call | solution.py:573
Async XLA Ops:
  0.6 58.9 %copy-start.1 = (f32[32,256]{1,0:T(8,128)S(1)}, f32[32,256]{1,0:T(8,128)}, u32[]{:S(2)}) copy-start(f32[32,256]{1,0:T(8,128)} %ow.1) | copy-start | bytes 98308
  0.7 58.9 %copy-start = (f32[64,128]{1,0:T(8,128)S(1)}, f32[64,128]{1,0:T(8,128)}, u32[]{:S(2)}) copy-start(f32[64,128]{1,0:T(8,128)} %qw.1) | copy-start | bytes 98308
